TPU v7x, 256 devices: a whole 4x4x8 slice. The times are simulated.
256 devices in a mesh: ep: 16 (over y, x), tp: 16 (over z, core).
Axes of the slice: x: 4, y: 4, z: 8, core: 2. Of those that a mesh axis runs over, the one named last changes fastest.
Arguments:
- mix_tokens: bfloat16 [16384, 1, 1024], P(('ep', 'tp')), may hold values from -6 to 6
- mix_gain: float32 [1024], replicated, may hold values from 0.1 to 1.9
- w_query: bfloat16 [1024, 1024], replicated, may hold values from -0.1875 to 0.1875
- w_key: bfloat16 [1024, 256], replicated, may hold values from -0.1875 to 0.1875
- w_value: bfloat16 [1024, 256], replicated, may hold values from -0.1875 to 0.1875
- query_gain: float32 [64], replicated, may hold values from 1.2 to 14
- key_gain: float32 [64], replicated, may hold values from 1.2 to 14
- w_out: bfloat16 [1024, 1024], replicated, may hold values from -0.1875 to 0.1875
- expert_tokens: bfloat16 [32768, 1024], P(('ep', 'tp')), may hold values from -6 to 6
- expert_gain: float32 [1024], replicated, may hold values from 0.1 to 1.9
- route_ids: int32 [32768, 2], P(('ep', 'tp')), may hold values from 0 to 31, all different within a row; in each aligned block of 128 rows (0 to 127, 128 to 255, ...) at most 9 rows name the same one
- route_weights: float32 [32768, 2], P(('ep', 'tp')), may hold values from 0.1 to 1
- w_gate: bfloat16 [32, 1024, 4096], P('ep', None, 'tp'), may hold values from -0.1875 to 0.1875
- w_up: bfloat16 [32, 1024, 4096], P('ep', None, 'tp'), may hold values from -0.1875 to 0.1875
- w_down: bfloat16 [32, 4096, 1024], P('ep', 'tp'), may hold values from -0.09375 to 0.09375
Outputs:
- mix_out: bfloat16 [16384, 1, 1024], P(('ep', 'tp'))
- experts_out: bfloat16 [32768, 1024], P(('ep', 'tp'))
Inputs may be any that keep to these rules, and one draw needn't show every extreme that they name: `route_ids`: each row names 2 different experts. Among the rows of one device no expert is named more than 9 times, and in every draw some expert is named exactly 9 times by the rows of some device.
All inputs are finite; a program needn't handle non-finite values.
Results may differ from a plain program's by a relative error of at most 0.018.
The roundings to bfloat16 on the way count: a program that leaves them out, or rounds other values in their place, can miss the bound.
Values may be sent and summed in bfloat16 or wider, within the bound.
A program may use at most 128 MiB of HBM per device.

v0:
```python
import math

import jax
import jax.numpy as jnp
from jax import lax
from jax.sharding import PartitionSpec as P

HEAD = 64
GRID_W = 64


epsilon = 1e-06


def normalize(values, gain_vec):
    widened = values.astype(jnp.float32)
    return (
        widened
        * lax.rsqrt(jnp.mean(widened * widened, axis=-1, keepdims=True) + epsilon)
        * gain_vec
    )


def angle_tables(positions, head_size):
    quarter = head_size // 4
    frequency = 10000.0 ** (-jnp.arange(quarter, dtype=jnp.float32) / quarter)
    grid_pos = jnp.stack([positions // GRID_W, positions % GRID_W], axis=-1).astype(jnp.float32)
    angles = grid_pos[:, :, None] * frequency[None, None, :]
    return (jnp.cos(angles), jnp.sin(angles))


def turn(values, cosine_table, sine_table):
    shaped = values.shape
    quarter = shaped[-1] // 4
    leading = (shaped[0],) + (1,) * (len(shaped) - 2) + (2, quarter)
    cosine_table = cosine_table.reshape(leading)
    sine_table = sine_table.reshape(leading)
    halves = values.reshape(shaped[:-1] + (2, 2, quarter))
    first_part = halves[..., 0, :]
    second_part = halves[..., 1, :]
    turned = jnp.stack(
        [
            first_part * cosine_table - second_part * sine_table,
            first_part * sine_table + second_part * cosine_table,
        ],
        axis=-2,
    )
    return turned.reshape(shaped)


def attend(queries, fold_state, key_piece):
    key_rows = key_piece.shape[0]
    block_rows = math.gcd(key_rows, 1024)
    blocks = key_piece.reshape((key_rows // block_rows, block_rows) + key_piece.shape[1:])
    score_scale = HEAD ** (-0.5)

    def step_block(carried, block_keys):
        running_max, totals, accumulated = carried
        keys_part = block_keys[..., :HEAD]
        values_part = block_keys[..., HEAD:]
        scores = (
            jnp.einsum("qshd,ksd->qshk", queries, keys_part, preferred_element_type=jnp.float32)
            * score_scale
        )
        new_max = jnp.maximum(running_max, jnp.max(scores, axis=-1))
        shrink = jnp.exp(running_max - new_max)
        raised = jnp.exp(scores - new_max[..., None])
        totals = totals * shrink + jnp.sum(raised, axis=-1)
        accumulated = accumulated * shrink[..., None] + jnp.einsum(
            "qshk,ksd->qshd",
            raised.astype(jnp.bfloat16),
            values_part,
            preferred_element_type=jnp.float32,
        )
        return ((new_max, totals, accumulated), None)

    return lax.scan(step_block, fold_state, blocks)[0]


def mixer_half(mix_tokens, mix_gain, w_query, w_key, w_value, query_gain, key_gain, w_out):
    tp_count = lax.axis_size("tp")
    seq_rows, sequences, model_width = mix_tokens.shape
    head_count = w_query.shape[1] // HEAD
    key_heads = w_key.shape[1] // HEAD
    local_heads = head_count // tp_count
    normed = normalize(mix_tokens, mix_gain).astype(jnp.bfloat16)
    queries = jnp.dot(normed, w_query, preferred_element_type=jnp.float32).astype(jnp.bfloat16)
    keys_raw = jnp.dot(normed, w_key, preferred_element_type=jnp.float32).astype(jnp.bfloat16)
    values = jnp.dot(normed, w_value, preferred_element_type=jnp.float32).astype(jnp.bfloat16)
    queries = queries.reshape(seq_rows, sequences, tp_count, local_heads * HEAD)
    key_value = jnp.concatenate(
        [
            keys_raw.reshape(seq_rows, sequences, key_heads, HEAD),
            values.reshape(seq_rows, sequences, key_heads, HEAD),
        ],
        axis=-1,
    )
    key_value = jnp.repeat(key_value, tp_count // key_heads, axis=2)
    packed = jnp.concatenate([queries, key_value], axis=-1)
    arrived = lax.all_to_all(packed, "tp", split_axis=2, concat_axis=0, tiled=True)
    span_rows = arrived.shape[0]
    positions = lax.axis_index("ep") * span_rows + jnp.arange(span_rows, dtype=jnp.int32)
    cosine_table, sine_table = angle_tables(positions, HEAD)
    query_width = local_heads * HEAD
    own_queries = normalize(
        arrived[:, :, 0, :query_width].reshape(span_rows, sequences, local_heads, HEAD), query_gain
    )
    own_queries = turn(own_queries, cosine_table, sine_table).astype(jnp.bfloat16)
    own_keys = normalize(arrived[:, :, 0, query_width : query_width + HEAD], key_gain)
    own_keys = turn(own_keys, cosine_table, sine_table).astype(jnp.bfloat16)
    key_pairs = jnp.concatenate([own_keys, arrived[:, :, 0, query_width + HEAD :]], axis=-1)
    start_state = (
        jnp.full((span_rows, sequences, local_heads), -1e30, jnp.float32),
        jnp.zeros((span_rows, sequences, local_heads), jnp.float32),
        jnp.zeros((span_rows, sequences, local_heads, HEAD), jnp.float32),
    )
    running_max, totals, accumulated = attend(
        own_queries, start_state, lax.all_gather(key_pairs, "ep", axis=0, tiled=True)
    )
    mixed = (
        (accumulated / totals[..., None])
        .astype(jnp.bfloat16)
        .reshape(span_rows, sequences, query_width)
    )
    returned = lax.all_to_all(mixed, "tp", split_axis=0, concat_axis=2, tiled=True)
    return jnp.dot(returned, w_out, preferred_element_type=jnp.float32).astype(jnp.bfloat16)


def joint_hidden(w_gate, w_up, piece_rows):
    gate_act = jnp.einsum("rjd,jdf->rjf", piece_rows, w_gate, preferred_element_type=jnp.float32)
    up_act = jnp.einsum("rjd,jdf->rjf", piece_rows, w_up, preferred_element_type=jnp.float32)
    return (jax.nn.silu(gate_act) * up_act).astype(jnp.bfloat16)


def joint_down(hidden_all, w_down):
    group_sum = jnp.einsum(
        "rjf,jfd->rjd", hidden_all, w_down, preferred_element_type=jnp.float32
    ).astype(jnp.bfloat16)
    return lax.optimization_barrier(group_sum).astype(jnp.float32)


def expert_half(expert_tokens, expert_gain, route_ids, route_weights, w_gate, w_up, w_down):
    ep_count = lax.axis_size("ep")
    tok_count, model_width = expert_tokens.shape
    top_count = route_ids.shape[1]
    local_experts = w_gate.shape[0]
    expert_count = local_experts * ep_count
    capacity = tok_count * top_count * 9 // (8 * expert_count)
    slot_count = ep_count * capacity * local_experts
    normed = normalize(expert_tokens, expert_gain).astype(jnp.bfloat16)
    flat_ids = route_ids.reshape(-1)
    matches = (flat_ids[:, None] == jnp.arange(expert_count, dtype=jnp.int32)[None, :]).astype(
        jnp.int32
    )
    rank_ids = jnp.sum((jnp.cumsum(matches, axis=0) - 1) * matches, axis=1)
    slot_ids = (
        flat_ids // local_experts * capacity + rank_ids
    ) * local_experts + flat_ids % local_experts
    chosen = slot_ids.reshape(tok_count, top_count)
    dispatch = jnp.sum(
        (chosen[:, :, None] == jnp.arange(slot_count, dtype=jnp.int32)[None, None, :]).astype(
            jnp.bfloat16
        ),
        axis=1,
    )
    outgoing = lax.dot_general(
        dispatch, normed, (((0,), (0,)), ((), ())), preferred_element_type=jnp.float32
    )
    outgoing = outgoing.astype(jnp.bfloat16).reshape(ep_count, capacity, local_experts, model_width)
    incoming = lax.all_to_all(outgoing, "ep", split_axis=0, concat_axis=0, tiled=True)
    own_rows = ep_count * capacity
    incoming = incoming.reshape(own_rows, local_experts, model_width)
    hidden_all = joint_hidden(w_gate, w_up, lax.all_gather(incoming, "tp", axis=0, tiled=True))
    summed = lax.psum_scatter(
        joint_down(hidden_all, w_down).astype(jnp.bfloat16), "tp", scatter_dimension=0, tiled=True
    )
    expert_results = summed.reshape(ep_count, capacity, local_experts, model_width)
    returned = lax.all_to_all(
        expert_results, "ep", split_axis=0, concat_axis=0, tiled=True
    ).reshape(slot_count, model_width)
    picked = jnp.take(returned, slot_ids, axis=0).reshape(tok_count, top_count, model_width)
    combined = jnp.sum(route_weights[:, :, None] * picked.astype(jnp.float32), axis=1)
    return combined.astype(jnp.bfloat16)


def body(
    mix_tokens,
    mix_gain,
    w_query,
    w_key,
    w_value,
    query_gain,
    key_gain,
    w_out,
    expert_tokens,
    expert_gain,
    route_ids,
    route_weights,
    w_gate,
    w_up,
    w_down,
):
    mix_out = mixer_half(mix_tokens, mix_gain, w_query, w_key, w_value, query_gain, key_gain, w_out)
    experts_out = expert_half(
        expert_tokens, expert_gain, route_ids, route_weights, w_gate, w_up, w_down
    )
    return (mix_out, experts_out)


def solution(mesh):
    placed = (
        P(("ep", "tp"), None, None),
        P(),
        P(),
        P(),
        P(),
        P(),
        P(),
        P(),
        P(("ep", "tp"), None),
        P(),
        P(("ep", "tp"), None),
        P(("ep", "tp"), None),
        P("ep", None, "tp"),
        P("ep", None, "tp"),
        P("ep", "tp", None),
    )
    return jax.shard_map(
        body,
        mesh=mesh,
        in_specs=placed,
        out_specs=(P(("ep", "tp"), None, None), P(("ep", "tp"), None)),
        check_vma=False,
    )
```

profile of v0, /device:TPU:1, one launch (start us, length us, event | category | flops | bytes accessed | tf_op | source)
XLA Modules:
  0.0 339.7 jit_solution(8806245419591874709)
XLA Ops:
  13.0 18.7 %all_to_all.43 = bf16[16,9,2,1024]{3,2,1,0:T(2,128)(2,1)S(1)} all-to-all(bf16[16,9,2,1024]{3,2,1,0:T(2,128)(2,1)S(1)} %reshape.571), channel_id=1, replica_groups=mesh['ep'=16,'tp'=16] {'ep'}, dimensions={0} | all-to-all | bytes 1179648 | tf_op jit(solution)/shard_map/all_to_all | solution.py:170
  37.7 10.4 %all-to-all-start = ((bf16[64,1,16,192]{3,0,1,2:T(8,128)(2,1)}), bf16[64,1,16,192]{3,0,1,2:T(8,128)(2,1)S(1)}, u32[]{:S(2)}, u32[]{:S(2)}) async-start(bf16[64,1,16,192]{3,0,1,2:T(8,128)(2,1)} %pad_maximum_fusion), calls=%async_computation | async-start | bytes 1048576 | tf_op jit(solution)/shard_map/all_to_all | solution.py:100
  48.3 22.1 %all-to-all-done = bf16[64,1,16,192]{3,0,1,2:T(8,128)(2,1)S(1)} async-done(((bf16[64,1,16,192]{3,0,1,2:T(8,128)(2,1)}), bf16[64,1,16,192]{3,0,1,2:T(8,128)(2,1)S(1)}, u32[]{:S(2)}, u32[]{:S(2)}) %all-to-all-start) | async-done | bytes 393248 | tf_op jit(solution)/shard_map/all_to_all | solution.py:100
  77.2 28.6 %all-gather.5.cloned.1.call-done = bf16[2304,2,1024]{2,0,1:T(8,128)(2,1)} async-done(((bf16[144,2,1024]{2,0,1:T(8,128)(2,1)}), bf16[2304,2,1024]{2,0,1:T(8,128)(2,1)}) %all-gather.5.cloned.1.call-update) | async-done | bytes 9437200 | tf_op jit(solution)/shard_map/all_gather | solution.py:173
  105.8 8.7 %convolution_bitcast_fusion.1 = f32[2304,2,256]{2,0,1:T(8,128)} fusion(bf16[2304,2,1024]{2,0,1:T(8,128)(2,1)} %all-gather.5.cloned.1.call-done, bf16[2,1024,256]{2,1,0:T(8,128)(2,1)} %param.29), kind=kOutput, calls=%fused_computation.26 | convolution fusion | flops 2415919104 | bytes 15204352 | tf_op jit(solution)/shard_map/rjd,jdf->rjf/dot_general | solution.py:130
  114.5 11.7 %convert_bitcast_fusion = bf16[2304,2,1024]{2,0,1:T(8,128)(2,1)} fusion(bf16[2,256,1024]{2,1,0:T(8,128)(2,1)} %param.31, bf16[2304,2,1024]{2,0,1:T(8,128)(2,1)} %all-gather.5.cloned.1.call-done, bf16[2,1024,256]{2,1,0:T(8,128)(2,1)} %param.30, f32[2304,2,256]{2,0,1:T(8,128)} %convolution_bitcast_fusion.1), kind=kOutput, calls=%fused_computation.23 | convolution fusion | flops 4843634688 | bytes 25690112 | tf_op jit(solution)/shard_map/rjf,jfd->rjd/dot_general | solution.py:136
  126.2 36.4 %all-gather.3.cloned.1.call-done = bf16[16384,1,128]{2,0,1:T(8,128)(2,1)} async-done(((bf16[1024,1,128]{2,0,1:T(8,128)(2,1)}), bf16[16384,1,128]{2,0,1:T(8,128)(2,1)}) %all-gather.3.cloned.1.call-update) | async-done | bytes 4194320 | tf_op jit(solution)/shard_map/all_gather | solution.py:118
  162.7 131.4 %while.15 = (s32[]{:T(128)}, f32[1024,1,1]{0,2,1:T(1,128)S(1)}, f32[1024,1,1]{0,2,1:T(1,128)S(1)}, f32[1024,1,1,64]{0,3,2,1:T(8,128)S(1)}, bf16[16,1024,1,128]{3...) while((s32[]{:T(128)}, f32[1024,1,1]{0,2,1:T(1,128)S(1)}, ...), condition=%wide.region_6.7_spmd.clone, body=%wide.region_3.6_spmd.clone.sunk | while | flops 277025792 | bytes 31129728 | solution.py:77
  166.4 3.1 fusion.81
  174.5 3.2 fusion.81
  183.0 3.2 fusion.81
  191.3 3.2 fusion.81
  199.6 3.2 fusion.81
  207.9 3.2 fusion.81
  213.5 2.7 multiply_reduce_fusion.4
  216.2 3.2 fusion.81
  224.5 3.2 fusion.81
  232.8 3.2 fusion.81
  238.3 2.7 multiply_reduce_fusion.4
  241.1 3.1 fusion.81
  249.2 3.1 fusion.81
  257.3 3.1 fusion.81
  262.6 2.7 multiply_reduce_fusion.4
  265.4 3.1 fusion.81
  273.5 3.1 fusion.81
  281.6 3.1 fusion.81
  289.7 3.1 fusion.81
  296.4 7.9 %all-to-all-start.1 = ((bf16[16,2,2048]{2,1,0:T(2,128)(2,1)}), bf16[16,2,2048]{2,1,0:T(2,128)(2,1)S(1)}, u32[]{:S(2)}, u32[]{:S(2)}) async-start(bf16[16,2,2048]{2,1,0:T(2,128)(2,1)} %reshape.590), calls=%async_computation.1 | async-start | bytes 262144 | tf_op jit(solution)/shard_map/all_to_all | solution.py:125
  307.1 6.0 %all-to-all-done.1 = bf16[16,2,2048]{2,1,0:T(2,128)(2,1)S(1)} async-done(((bf16[16,2,2048]{2,1,0:T(2,128)(2,1)}), bf16[16,2,2048]{2,1,0:T(2,128)(2,1)S(1)}, u32[]{:S(2)}, u32[]{:S(2)}) %all-to-all-start.1) | async-done | bytes 131104 | tf_op jit(solution)/shard_map/all_to_all | solution.py:125
  313.1 4.2 %all-to-all-start.3 = ((bf16[16,9,2,1024]{3,2,1,0:T(2,128)(2,1)}), bf16[16,9,2,1024]{3,2,1,0:T(2,128)(2,1)S(1)}, u32[]{:S(2)}, u32[]{:S(2)}) async-start(bf16[16,9,2,1024]{3,2,1,0:T(2,128)(2,1)} %bitcast.24), calls=%async_computation.4 | async-start | bytes 1179648 | tf_op jit(solution)/shard_map/all_to_all | solution.py:178
  318.8 2.7 fusion.20
  321.5 7.7 %all-to-all-done.3 = bf16[16,9,2,1024]{3,2,1,0:T(2,128)(2,1)S(1)} async-done(((bf16[16,9,2,1024]{3,2,1,0:T(2,128)(2,1)}), bf16[16,9,2,1024]{3,2,1,0:T(2,128)(2,1)S(1)}, u32[]{:S(2)}, u32[]{:S(2)}) %all-to-all-start.3) | async-done | bytes 589856 | tf_op jit(solution)/shard_map/all_to_all | solution.py:178
  (217 shorter events, 101.8 us)
Async XLA Ops:
  7.2 28.7 %copy-start = (bf16[1024,1024]{1,0:T(8,128)(2,1)S(1)}, bf16[1024,1024]{1,0:T(8,128)(2,1)}, u32[]{:S(2)}) copy-start(bf16[1024,1024]{1,0:T(8,128)(2,1)} %param.19) | copy-start | bytes 6291460
  7.2 25.5 %copy-start.2 = (bf16[64,1,1024]{2,0,1:T(8,128)(2,1)S(1)}, bf16[64,1,1024]{2,0,1:T(8,128)(2,1)}, u32[]{:S(2)}) copy-start(bf16[64,1,1024]{2,0,1:T(8,128)(2,1)} %param.17) | copy-start | bytes 393220
  7.2 25.7 %copy-start.3 = (f32[1024]{0:T(1024)S(1)}, f32[1024]{0:T(1024)}, u32[]{:S(2)}) copy-start(f32[1024]{0:T(1024)} %param.18) | copy-start | bytes 12292
  7.2 98.6 %all-gather.5.cloned.1.call-start = ((), (), s32[]{:S(2)}) async-start(), calls=%async_computation.6 | async-start | bytes 10027008 | tf_op jit(solution)/shard_map/all_gather | solution.py:173
  32.7 15.4 %copy-start.6 = (f32[64]{0:T(128)S(1)}, f32[64]{0:T(128)}, u32[]{:S(2)}) copy-start(f32[64]{0:T(128)} %param.23) | copy-start | bytes 772
  36.7 39.9 %copy-start.5 = (f32[64]{0:T(128)S(1)}, f32[64]{0:T(128)}, u32[]{:S(2)}) copy-start(f32[64]{0:T(128)} %param.22) | copy-start | bytes 772
  37.7 32.7 %all-to-all-start = ((bf16[64,1,16,192]{3,0,1,2:T(8,128)(2,1)}), bf16[64,1,16,192]{3,0,1,2:T(8,128)(2,1)S(1)}, u32[]{:S(2)}, u32[]{:S(2)}) async-start(bf16[64,1,16,192]{3,0,1,2:T(8,128)(2,1)} %pad_maximum_fusion), calls=%async_computation | async-start | bytes 1048576 | tf_op jit(solution)/shard_map/all_to_all | solution.py:100
  48.1 114.6 %all-gather.3.cloned.1.call-start = ((), (), s32[]{:S(2)}) async-start(), calls=%async_computation.5 | async-start | bytes 4456448 | tf_op jit(solution)/shard_map/all_gather | solution.py:118
  75.1 229.5 %reduce-scatter.2.cloned.1.call-start = ((), (), s32[]{:S(2)}) async-start(), calls=%async_computation.7 | async-start | bytes 10027008 | tf_op jit(solution)/shard_map/reduce_scatter | solution.py:174
  162.7 141.9 %copy-start.4 = (f32[128,2]{0,1:T(2,128)S(1)}, f32[128,2]{0,1:T(2,128)}, u32[]{:S(2)}) copy-start(f32[128,2]{0,1:T(2,128)} %param.28) | copy-start | bytes 3076
  166.4 3.4 %copy-start.1 = (f32[1024,1024]{1,0:T(8,128)S(1)}, f32[1024,1024]{1,0:T(8,128)}, u32[]{:S(2)}) copy-start(f32[1024,1024]{1,0:T(8,128)} %get-tuple-element.163) | copy-start | bytes 12582916 | tf_op jit(solution)/shard_map/while
  174.5 3.9 %copy-start.1 = (f32[1024,1024]{1,0:T(8,128)S(1)}, f32[1024,1024]{1,0:T(8,128)}, u32[]{:S(2)}) copy-start(f32[1024,1024]{1,0:T(8,128)} %get-tuple-element.163) | copy-start | bytes 12582916 | tf_op jit(solution)/shard_map/while
  183.0 3.6 %copy-start.1 = (f32[1024,1024]{1,0:T(8,128)S(1)}, f32[1024,1024]{1,0:T(8,128)}, u32[]{:S(2)}) copy-start(f32[1024,1024]{1,0:T(8,128)} %get-tuple-element.163) | copy-start | bytes 12582916 | tf_op jit(solution)/shard_map/while
  191.3 3.6 %copy-start.1 = (f32[1024,1024]{1,0:T(8,128)S(1)}, f32[1024,1024]{1,0:T(8,128)}, u32[]{:S(2)}) copy-start(f32[1024,1024]{1,0:T(8,128)} %get-tuple-element.163) | copy-start | bytes 12582916 | tf_op jit(solution)/shard_map/while
  199.6 3.6 %copy-start.1 = (f32[1024,1024]{1,0:T(8,128)S(1)}, f32[1024,1024]{1,0:T(8,128)}, u32[]{:S(2)}) copy-start(f32[1024,1024]{1,0:T(8,128)} %get-tuple-element.163) | copy-start | bytes 12582916 | tf_op jit(solution)/shard_map/while
  207.9 3.6 %copy-start.1 = (f32[1024,1024]{1,0:T(8,128)S(1)}, f32[1024,1024]{1,0:T(8,128)}, u32[]{:S(2)}) copy-start(f32[1024,1024]{1,0:T(8,128)} %get-tuple-element.163) | copy-start | bytes 12582916 | tf_op jit(solution)/shard_map/while
  216.2 3.6 %copy-start.1 = (f32[1024,1024]{1,0:T(8,128)S(1)}, f32[1024,1024]{1,0:T(8,128)}, u32[]{:S(2)}) copy-start(f32[1024,1024]{1,0:T(8,128)} %get-tuple-element.163) | copy-start | bytes 12582916 | tf_op jit(solution)/shard_map/while
  224.5 3.6 %copy-start.1 = (f32[1024,1024]{1,0:T(8,128)S(1)}, f32[1024,1024]{1,0:T(8,128)}, u32[]{:S(2)}) copy-start(f32[1024,1024]{1,0:T(8,128)} %get-tuple-element.163) | copy-start | bytes 12582916 | tf_op jit(solution)/shard_map/while
  232.8 3.6 %copy-start.1 = (f32[1024,1024]{1,0:T(8,128)S(1)}, f32[1024,1024]{1,0:T(8,128)}, u32[]{:S(2)}) copy-start(f32[1024,1024]{1,0:T(8,128)} %get-tuple-element.163) | copy-start | bytes 12582916 | tf_op jit(solution)/shard_map/while
  241.0 3.4 %copy-start.1 = (f32[1024,1024]{1,0:T(8,128)S(1)}, f32[1024,1024]{1,0:T(8,128)}, u32[]{:S(2)}) copy-start(f32[1024,1024]{1,0:T(8,128)} %get-tuple-element.163) | copy-start | bytes 12582916 | tf_op jit(solution)/shard_map/while
  249.1 3.4 %copy-start.1 = (f32[1024,1024]{1,0:T(8,128)S(1)}, f32[1024,1024]{1,0:T(8,128)}, u32[]{:S(2)}) copy-start(f32[1024,1024]{1,0:T(8,128)} %get-tuple-element.163) | copy-start | bytes 12582916 | tf_op jit(solution)/shard_map/while
  257.2 3.4 %copy-start.1 = (f32[1024,1024]{1,0:T(8,128)S(1)}, f32[1024,1024]{1,0:T(8,128)}, u32[]{:S(2)}) copy-start(f32[1024,1024]{1,0:T(8,128)} %get-tuple-element.163) | copy-start | bytes 12582916 | tf_op jit(solution)/shard_map/while
  265.4 3.4 %copy-start.1 = (f32[1024,1024]{1,0:T(8,128)S(1)}, f32[1024,1024]{1,0:T(8,128)}, u32[]{:S(2)}) copy-start(f32[1024,1024]{1,0:T(8,128)} %get-tuple-element.163) | copy-start | bytes 12582916 | tf_op jit(solution)/shard_map/while
  273.5 3.4 %copy-start.1 = (f32[1024,1024]{1,0:T(8,128)S(1)}, f32[1024,1024]{1,0:T(8,128)}, u32[]{:S(2)}) copy-start(f32[1024,1024]{1,0:T(8,128)} %get-tuple-element.163) | copy-start | bytes 12582916 | tf_op jit(solution)/shard_map/while
  281.6 3.4 %copy-start.1 = (f32[1024,1024]{1,0:T(8,128)S(1)}, f32[1024,1024]{1,0:T(8,128)}, u32[]{:S(2)}) copy-start(f32[1024,1024]{1,0:T(8,128)} %get-tuple-element.163) | copy-start | bytes 12582916 | tf_op jit(solution)/shard_map/while
  289.7 3.4 %copy-start.1 = (f32[1024,1024]{1,0:T(8,128)S(1)}, f32[1024,1024]{1,0:T(8,128)}, u32[]{:S(2)}) copy-start(f32[1024,1024]{1,0:T(8,128)} %get-tuple-element.163) | copy-start | bytes 12582916 | tf_op jit(solution)/shard_map/while
  296.4 16.8 %all-to-all-start.1 = ((bf16[16,2,2048]{2,1,0:T(2,128)(2,1)}), bf16[16,2,2048]{2,1,0:T(2,128)(2,1)S(1)}, u32[]{:S(2)}, u32[]{:S(2)}) async-start(bf16[16,2,2048]{2,1,0:T(2,128)(2,1)} %reshape.590), calls=%async_computation.1 | async-start | bytes 262144 | tf_op jit(solution)/shard_map/all_to_all | solution.py:125
  313.1 16.1 %all-to-all-start.3 = ((bf16[16,9,2,1024]{3,2,1,0:T(2,128)(2,1)}), bf16[16,9,2,1024]{3,2,1,0:T(2,128)(2,1)S(1)}, u32[]{:S(2)}, u32[]{:S(2)}) async-start(bf16[16,9,2,1024]{3,2,1,0:T(2,128)(2,1)} %bitcast.24), calls=%async_computation.4 | async-start | bytes 1179648 | tf_op jit(solution)/shard_map/all_to_all | solution.py:178
Sparse Core Ops, SparseCore 0:
  32.8 72.8 all-gather.4
  108.2 54.3 all-gather.2
  165.2 69.8 reduce-scatter.1
where the time goes:
time: 341 us; the launch traced here: 340 us
  waiting for transfers between devices  101 us (30%)
  matrix products  85.9 us (25%)
  other arithmetic  61.8 us (18%)
  local copies, waits for them, and re-layouts  35 us (10%)
  starting transfers between devices  22.7 us (7%)
  blocking collectives  18.7 us (5%)
  between operations  14.2 us (4%)
    reduce_sum x16, other arithmetic, step_block(): totals = totals * shrink + jnp.sum(raised, axis=-1)  50 us
    dot_general x16, matrix products, step_block(): jnp.einsum('qshd,ksd->qshk', queries, keys_part, preferred_element_type=j...  43.4 us
    all_gather x1, waiting for transfers between devices, mixer_half(): lax.all_gather(key_pairs, 'ep', axis=0, tiled=True)  36.4 us
    all_gather x1, waiting for transfers between devices, expert_half(): lax.all_gather(incoming, 'tp', axis=0, tiled=True)  28.6 us
    all_to_all x1, waiting for transfers between devices, mixer_half(): lax.all_to_all(packed, 'tp', split_axis=2, concat_axis=0, tiled=True)  22.1 us
    all_to_all x1, blocking collectives, expert_half(): lax.all_to_all(outgoing, 'ep', split_axis=0, concat_axis=0, tiled=True)  18.7 us
    squeeze x16, local copies, waits for them, and re-layouts, attend(): return lax.scan(step_block, fold_state, blocks)[0]  15.6 us
    dot_general x16, matrix products, step_block(): jnp.einsum('qshk,ksd->qshd', raised.astype(jnp.bfloat16), values_part, pr...  14.9 us
  transfers between devices with their start and end apart: 6, of which 5 were waited for; matrix products, arithmetic and copies ran while one was open for 49% of the time, Pallas kernels for 0%

commit v1 on v0

v1 whole, which is shorter than its diff:
```python
import functools
import math

import jax
import jax.numpy as jnp
from jax import lax
from jax.experimental import pallas as pl
from jax.experimental.pallas import tpu as pltpu
from jax.sharding import PartitionSpec as P

HEAD = 64
GRID_W = 64
EXP2_SCALE = HEAD ** (-0.5) * math.log2(math.e)
MESH = pl.DeviceIdType.MESH
MIB = 1024 * 1024


epsilon = 1e-06


def normalize(values, gain_vec):
    widened = values.astype(jnp.float32)
    return (
        widened
        * lax.rsqrt(jnp.mean(widened * widened, axis=-1, keepdims=True) + epsilon)
        * gain_vec
    )


def angle_tables(positions, head_size):
    quarter = head_size // 4
    frequency = 10000.0 ** (-jnp.arange(quarter, dtype=jnp.float32) / quarter)
    grid_pos = jnp.stack([positions // GRID_W, positions % GRID_W], axis=-1).astype(jnp.float32)
    angles = grid_pos[:, :, None] * frequency[None, None, :]
    return (jnp.cos(angles), jnp.sin(angles))


def turn(values, cosine_table, sine_table):
    shaped = values.shape
    quarter = shaped[-1] // 4
    leading = (shaped[0],) + (1,) * (len(shaped) - 2) + (2, quarter)
    cosine_table = cosine_table.reshape(leading)
    sine_table = sine_table.reshape(leading)
    halves = values.reshape(shaped[:-1] + (2, 2, quarter))
    first_part = halves[..., 0, :]
    second_part = halves[..., 1, :]
    turned = jnp.stack(
        [
            first_part * cosine_table - second_part * sine_table,
            first_part * sine_table + second_part * cosine_table,
        ],
        axis=-2,
    )
    return turned.reshape(shaped)


def meet(peers):
    barrier = pltpu.get_barrier_semaphore()
    for peer in peers:
        pl.semaphore_signal(barrier, inc=1, device_id=peer, device_id_type=MESH)
    pl.semaphore_wait(barrier, len(peers))


def exchange_body(x_ref, y_ref, x_out, y_out, x_send, x_recv, y_send, y_recv):
    lanes = []
    for axis, source, target, send, recv in (
        ("tp", y_ref, y_out, y_send, y_recv),
        ("ep", x_ref, x_out, x_send, x_recv),
    ):
        lanes.append((axis, lax.axis_index(axis), source.shape[0], source, target, send, recv))
    meet([{axis: lax.rem(me + d, n)} for axis, me, n, *_ in lanes for d in range(1, n)])
    copies = []
    for axis, me, n, source, target, send, recv in lanes:
        for d in range(1, n):
            peer = lax.rem(me + d, n)
            copy = pltpu.make_async_remote_copy(
                src_ref=source.at[peer],
                dst_ref=target.at[me],
                send_sem=send.at[d],
                recv_sem=recv.at[d],
                device_id={axis: peer},
                device_id_type=MESH,
            )
            copy.start()
            copies.append(copy)
    for axis, me, n, source, target, send, recv in lanes:
        target[me] = source[me]
    for copy in copies:
        copy.wait()


def exchange(x, y, collective_id):
    vmem = pl.BlockSpec(memory_space=pltpu.VMEM)
    x_count, y_count = x.shape[0], y.shape[0]
    return pl.pallas_call(
        exchange_body,
        out_shape=[jax.ShapeDtypeStruct(a.shape, a.dtype) for a in (x, y)],
        in_specs=[vmem, vmem],
        out_specs=[vmem, vmem],
        scratch_shapes=[
            pltpu.SemaphoreType.DMA((x_count,)),
            pltpu.SemaphoreType.DMA((x_count,)),
            pltpu.SemaphoreType.DMA((y_count,)),
            pltpu.SemaphoreType.DMA((y_count,)),
        ],
        name="exchange",
        cost_estimate=pl.CostEstimate(flops=10**10, bytes_accessed=10**6, transcendentals=0),
        compiler_params=pltpu.CompilerParams(
            collective_id=collective_id, has_side_effects=True, vmem_limit_bytes=24 * MIB
        ),
    )(x, y)


def ring_places():
    me = lax.axis_index("tp")
    chips = lax.axis_size("tp") // 2
    chip, core = me // 2, lax.rem(me, 2)
    ahead = lax.rem(chip + 1 - 2 * core + chips, chips) * 2 + core
    behind = lax.rem(chip - 1 + 2 * core + chips, chips) * 2 + core
    partner = chip * 2 + 1 - core
    return {"tp": ahead}, {"tp": behind}, {"tp": partner}


def gather_body(
    rows_ref,
    gate_ref,
    up_ref,
    down_ref,
    own_out,
    pair_out,
    held,
    own_part,
    pair_part,
    load_sem,
    ring_send,
    ring_recv,
    pair_send,
    pair_recv,
    own_sem,
    part_send,
    part_recv,
):
    pieces, _, piece_rows, width = held.shape
    ahead, behind, partner = ring_places()
    loads = [
        pltpu.make_async_copy(rows_ref.at[j], held.at[j, 0], load_sem.at[j]) for j in range(2)
    ]
    for load in loads:
        load.start()

    def ring_copy(i):
        return pltpu.make_async_remote_copy(
            src_ref=held.at[i, 0],
            dst_ref=held.at[i + 2, 0],
            send_sem=ring_send.at[i],
            recv_sem=ring_recv.at[i + 2],
            device_id=ahead,
            device_id_type=MESH,
        )

    def ring_arrival(i):
        return pltpu.make_async_remote_copy(
            src_ref=held.at[i, 0],
            dst_ref=held.at[i, 0],
            send_sem=ring_send.at[i],
            recv_sem=ring_recv.at[i],
            device_id=ahead,
            device_id_type=MESH,
        )

    def pair_copy(i):
        return pltpu.make_async_remote_copy(
            src_ref=held.at[i, 0],
            dst_ref=held.at[i, 1],
            send_sem=pair_send.at[i],
            recv_sem=pair_recv.at[i],
            device_id=partner,
            device_id_type=MESH,
        )

    def part_copy(i):
        return pltpu.make_async_remote_copy(
            src_ref=pair_part.at[i],
            dst_ref=pair_out.at[i],
            send_sem=part_send.at[i],
            recv_sem=part_recv.at[i],
            device_id=partner,
            device_id_type=MESH,
        )

    def own_copy(i):
        return pltpu.make_async_copy(own_part.at[i], own_out.at[i], own_sem.at[i])

    meet([ahead, behind, partner])
    for load in loads:
        load.wait()

    def step(i, _):
        @pl.when(i < pieces)
        def _():
            @pl.when(i >= 2)
            def _():
                ring_arrival(i).wait_recv()

            @pl.when(i < pieces - 2)
            def _():
                ring_copy(i).start()

            pair_copy(i).start()

        @pl.when(jnp.logical_and(i >= 1, i <= pieces))
        def _():
            piece = i - 1
            expert = lax.rem(piece, 2)
            pair_copy(piece).wait_recv()
            rows = held[piece].reshape(2 * piece_rows, width)
            gate_act = jnp.dot(rows, gate_ref[expert], preferred_element_type=jnp.float32)
            up_act = jnp.dot(rows, up_ref[expert], preferred_element_type=jnp.float32)
            hidden = (gate_act / (1.0 + jnp.exp(-gate_act)) * up_act).astype(jnp.bfloat16)
            sums = jnp.dot(hidden, down_ref[expert], preferred_element_type=jnp.float32)
            sums = sums.astype(jnp.bfloat16)
            own_part[piece] = sums[:piece_rows]
            pair_part[piece] = sums[piece_rows:]

        @pl.when(i >= 2)
        def _():
            own_copy(i - 2).start()
            part_copy(i - 2).start()

        return 0

    lax.fori_loop(0, pieces + 2, step, 0)

    def finish(i, _):
        @pl.when(i < pieces - 2)
        def _():
            ring_copy(i).wait_send()

        pair_copy(i).wait_send()
        own_copy(i).wait()
        part_copy(i).wait()
        return 0

    lax.fori_loop(0, pieces, finish, 0)


def gather_experts(rows, w_gate, w_up, w_down):
    pieces = lax.axis_size("tp")
    _, piece_rows, width = rows.shape
    vmem, hbm = pl.BlockSpec(memory_space=pltpu.VMEM), pl.BlockSpec(memory_space=pl.ANY)
    part = jax.ShapeDtypeStruct((pieces, piece_rows, width), jnp.bfloat16)
    dma = pltpu.SemaphoreType.DMA
    return pl.pallas_call(
        gather_body,
        out_shape=[part, part],
        in_specs=[hbm, vmem, vmem, vmem],
        out_specs=[hbm, hbm],
        scratch_shapes=[
            pltpu.VMEM((pieces, 2, piece_rows, width), jnp.bfloat16),
            pltpu.VMEM((pieces, piece_rows, width), jnp.bfloat16),
            pltpu.VMEM((pieces, piece_rows, width), jnp.bfloat16),
            dma((2,)),
        ]
        + [dma((pieces,)) for _ in range(7)],
        name="gather_experts",
        cost_estimate=pl.CostEstimate(
            flops=5 * 10**10, bytes_accessed=2 * 10**7, transcendentals=0
        ),
        compiler_params=pltpu.CompilerParams(
            collective_id=1, has_side_effects=True, vmem_limit_bytes=44 * MIB
        ),
    )(rows, w_gate, w_up, w_down)


def scatter_body(
    query_tile,
    key_block,
    query_ref,
    pair_ref,
    own_hbm,
    part_hbm,
    sums_out,
    mixed_out,
    own_part,
    pair_part,
    arrived,
    leaving,
    row_max,
    row_sum,
    row_acc,
    own_sem,
    part_sem,
    ring_send,
    ring_recv,
):
    pieces = own_part.shape[0]
    tiles, blocks = query_ref.shape[0] // query_tile, pair_ref.shape[0] // key_block
    slices = tiles * blocks // pieces
    ahead, behind, _ = ring_places()

    def loads(i):
        slot = lax.rem(i + 2, pieces)
        return (
            pltpu.make_async_copy(own_hbm.at[slot], own_part.at[i], own_sem.at[i]),
            pltpu.make_async_copy(part_hbm.at[slot], pair_part.at[i], part_sem.at[i]),
        )

    def ring_copy(i):
        return pltpu.make_async_remote_copy(
            src_ref=leaving.at[i],
            dst_ref=arrived.at[i],
            send_sem=ring_send.at[i],
            recv_sem=ring_recv.at[i],
            device_id=ahead,
            device_id_type=MESH,
        )

    def start_loads(i, _):
        for load in loads(i):
            load.start()
        return 0

    lax.fori_loop(0, pieces, start_loads, 0)
    meet([ahead, behind])
    row_max[...] = jnp.full(row_max.shape, -1e30, jnp.float32)
    row_sum[...] = jnp.zeros(row_sum.shape, jnp.float32)
    row_acc[...] = jnp.zeros(row_acc.shape, jnp.float32)

    def attend_slice(number):
        block, tile = number // tiles, lax.rem(number, tiles)
        first = pl.multiple_of(tile * query_tile, query_tile)
        queries = query_ref[pl.ds(first, query_tile), :]
        pairs = pair_ref[pl.ds(pl.multiple_of(block * key_block, key_block), key_block), :]
        scores = lax.dot_general(
            queries, pairs, (((1,), (1,)), ((), ())), preferred_element_type=jnp.float32
        )
        old_max = row_max[tile][:, :1]
        new_max = jnp.maximum(old_max, jnp.max(scores, axis=1, keepdims=True))
        shrink = jnp.exp2((old_max - new_max) * EXP2_SCALE)
        raised = jnp.exp2((scores - new_max) * EXP2_SCALE)
        lane_sums = raised[:, :128]
        for lane in range(128, key_block, 128):
            lane_sums = lane_sums + raised[:, lane : lane + 128]
        row_max[tile] = jnp.broadcast_to(new_max, (query_tile, 128))
        row_sum[tile] = row_sum[tile] * shrink + lane_sums
        row_acc[tile] = row_acc[tile] * shrink + jnp.dot(
            raised.astype(jnp.bfloat16), pairs, preferred_element_type=jnp.float32
        )

    def step(i, _):
        for load in loads(i):
            load.wait()

        @pl.when(i < 2)
        def _():
            total = own_part[i].astype(jnp.float32) + pair_part[i].astype(jnp.float32)
            leaving[i] = total.astype(jnp.bfloat16)

        @pl.when(i >= 2)
        def _():
            ring_copy(i - 2).wait_recv()
            total = own_part[i].astype(jnp.float32) + pair_part[i].astype(jnp.float32)
            total = (total + arrived[i - 2].astype(jnp.float32)).astype(jnp.bfloat16)

            @pl.when(i < pieces - 2)
            def _():
                leaving[i] = total

            @pl.when(i >= pieces - 2)
            def _():
                sums_out[i - (pieces - 2)] = total

        @pl.when(i < pieces - 2)
        def _():
            ring_copy(i).start()

        for part in range(slices):
            attend_slice(i * slices + part)
        return 0

    lax.fori_loop(0, pieces, step, 0)

    def finish(i, _):
        ring_copy(i).wait_send()
        return 0

    lax.fori_loop(0, pieces - 2, finish, 0)
    for tile in range(tiles):
        mixed = row_acc[tile] / jnp.sum(row_sum[tile], axis=1, keepdims=True)
        mixed_out[tile * query_tile : (tile + 1) * query_tile, :] = mixed.astype(jnp.bfloat16)


def scatter_experts(queries, pairs, own_part, pair_part):
    pieces, piece_rows, width = own_part.shape
    rows, keys = queries.shape[0], pairs.shape[0]
    query_tile, key_block = math.gcd(rows, 256), math.gcd(keys, 2048)
    tiles = rows // query_tile
    vmem, hbm = pl.BlockSpec(memory_space=pltpu.VMEM), pl.BlockSpec(memory_space=pl.ANY)
    dma = pltpu.SemaphoreType.DMA
    piece = (piece_rows, width)
    return pl.pallas_call(
        functools.partial(scatter_body, query_tile, key_block),
        out_shape=[
            jax.ShapeDtypeStruct((2,) + piece, jnp.bfloat16),
            jax.ShapeDtypeStruct((rows, 2 * HEAD), jnp.bfloat16),
        ],
        in_specs=[vmem, vmem, hbm, hbm],
        out_specs=[vmem, vmem],
        scratch_shapes=[
            pltpu.VMEM((pieces,) + piece, jnp.bfloat16),
            pltpu.VMEM((pieces,) + piece, jnp.bfloat16),
            pltpu.VMEM((pieces - 2,) + piece, jnp.bfloat16),
            pltpu.VMEM((pieces - 2,) + piece, jnp.bfloat16),
            pltpu.VMEM((tiles, query_tile, 128), jnp.float32),
            pltpu.VMEM((tiles, query_tile, 128), jnp.float32),
            pltpu.VMEM((tiles, query_tile, 128), jnp.float32),
            dma((pieces,)),
            dma((pieces,)),
            dma((pieces,)),
            dma((pieces,)),
        ],
        name="scatter_experts",
        cost_estimate=pl.CostEstimate(
            flops=5 * 10**10, bytes_accessed=2 * 10**7, transcendentals=0
        ),
        compiler_params=pltpu.CompilerParams(
            collective_id=2, has_side_effects=True, vmem_limit_bytes=52 * MIB
        ),
    )(queries, pairs, own_part, pair_part)


def body(
    mix_tokens,
    mix_gain,
    w_query,
    w_key,
    w_value,
    query_gain,
    key_gain,
    w_out,
    expert_tokens,
    expert_gain,
    route_ids,
    route_weights,
    w_gate,
    w_up,
    w_down,
):
    tp_count, ep_count = lax.axis_size("tp"), lax.axis_size("ep")
    seq_rows, sequences, model_width = mix_tokens.shape
    key_heads = w_key.shape[1] // HEAD
    half_rows = seq_rows // 2
    mix_normed = normalize(mix_tokens[:, 0, :], mix_gain).astype(jnp.bfloat16)
    queries = jnp.dot(mix_normed, w_query, preferred_element_type=jnp.float32).astype(jnp.bfloat16)
    keys_raw = jnp.dot(mix_normed, w_key, preferred_element_type=jnp.float32).astype(jnp.bfloat16)
    values = jnp.dot(mix_normed, w_value, preferred_element_type=jnp.float32).astype(jnp.bfloat16)
    by_head = queries.reshape(2, half_rows, tp_count, HEAD)
    by_head = jnp.transpose(by_head, (2, 1, 0, 3)).reshape(tp_count, half_rows, 2 * HEAD)
    key_value = jnp.concatenate(
        [keys_raw.reshape(seq_rows, key_heads, HEAD), values.reshape(seq_rows, key_heads, HEAD)],
        axis=-1,
    )
    key_value = jnp.repeat(jnp.transpose(key_value, (1, 0, 2)), tp_count // key_heads, axis=0)
    packed = jnp.concatenate([key_value, by_head], axis=1)

    tok_count = expert_tokens.shape[0]
    top_count = route_ids.shape[1]
    local_experts = w_gate.shape[0]
    expert_count = local_experts * ep_count
    capacity = tok_count * top_count * 9 // (8 * expert_count)
    slot_count = ep_count * capacity * local_experts
    normed = normalize(expert_tokens, expert_gain).astype(jnp.bfloat16)
    flat_ids = route_ids.reshape(-1)
    matches = (flat_ids[:, None] == jnp.arange(expert_count, dtype=jnp.int32)[None, :]).astype(
        jnp.int32
    )
    rank_ids = jnp.sum((jnp.cumsum(matches, axis=0) - 1) * matches, axis=1)
    slot_ids = (
        flat_ids // local_experts * local_experts + flat_ids % local_experts
    ) * capacity + rank_ids
    chosen = slot_ids.reshape(tok_count, top_count)
    slots = jnp.arange(slot_count, dtype=jnp.int32)
    hits = chosen[:, :, None] == slots[None, None, :]
    dispatch = jnp.sum(hits.astype(jnp.bfloat16), axis=1)
    outgoing = lax.dot_general(
        dispatch, normed, (((0,), (0,)), ((), ())), preferred_element_type=jnp.float32
    ).astype(jnp.bfloat16)
    lane_rows = local_experts * capacity * model_width // 128
    outgoing = outgoing.reshape(ep_count, lane_rows, 128)

    incoming, arrived = exchange(outgoing, packed, 0)

    span_rows = tp_count * seq_rows
    positions = lax.axis_index("ep") * span_rows + jnp.arange(span_rows, dtype=jnp.int32)
    cosine_table, sine_table = angle_tables(positions, HEAD)
    pair_rows = arrived[:, :seq_rows, :].reshape(span_rows, 2 * HEAD)
    own_queries = arrived[:, seq_rows:, :].reshape(tp_count, half_rows, 2, HEAD)
    own_queries = jnp.transpose(own_queries, (0, 2, 1, 3)).reshape(span_rows, HEAD)
    own_queries = turn(normalize(own_queries, query_gain), cosine_table, sine_table)
    padded_queries = jnp.pad(own_queries.astype(jnp.bfloat16), ((0, 0), (0, HEAD)))
    own_keys = turn(normalize(pair_rows[:, :HEAD], key_gain), cosine_table, sine_table)
    key_pairs = jnp.concatenate([own_keys.astype(jnp.bfloat16), pair_rows[:, HEAD:]], axis=-1)
    pairs = lax.all_gather(key_pairs, "ep", axis=0, tiled=True)

    own_rows = ep_count * capacity
    rows = incoming.reshape(ep_count, local_experts, capacity, model_width)
    rows = jnp.transpose(rows, (1, 0, 2, 3)).reshape(local_experts, own_rows, model_width)
    own_part, pair_part = gather_experts(rows, w_gate, w_up, w_down)
    summed, mixed = scatter_experts(padded_queries, pairs, own_part, pair_part)

    summed = summed.reshape(local_experts, ep_count, capacity, model_width)
    summed = jnp.transpose(summed, (1, 0, 2, 3)).reshape(ep_count, lane_rows, 128)
    results, heads = exchange(summed, mixed.reshape(tp_count, seq_rows, 2 * HEAD), 3)

    heads = jnp.transpose(heads[:, :, HEAD:], (1, 0, 2)).reshape(seq_rows, tp_count * HEAD)
    mix_out = jnp.dot(heads, w_out, preferred_element_type=jnp.float32).astype(jnp.bfloat16)
    results = results.reshape(slot_count, model_width)
    picked = jnp.take(results, slot_ids, axis=0).reshape(tok_count, top_count, model_width)
    combined = jnp.sum(route_weights[:, :, None] * picked.astype(jnp.float32), axis=1)
    return (mix_out[:, None, :], combined.astype(jnp.bfloat16))


def solution(mesh):
    placed = (
        P(("ep", "tp"), None, None),
        P(),
        P(),
        P(),
        P(),
        P(),
        P(),
        P(),
        P(("ep", "tp"), None),
        P(),
        P(("ep", "tp"), None),
        P(("ep", "tp"), None),
        P("ep", None, "tp"),
        P("ep", None, "tp"),
        P("ep", "tp", None),
    )
    return jax.shard_map(
        body,
        mesh=mesh,
        in_specs=placed,
        out_specs=(P(("ep", "tp"), None, None), P(("ep", "tp"), None)),
        check_vma=False,
    )
```

time: 341 us -> 211 us (0.62)
  Pallas kernels: 0 us -> 146 us
  waiting for transfers between devices: 101 us -> 0.02 us
  matrix products: 85.9 us -> 7.18 us
  other arithmetic: 61.8 us -> 13.1 us
  starting transfers between devices: 22.7 us -> 0.04 us
  blocking collectives: 18.7 us -> 0 us
  local copies, waits for them, and re-layouts: 35 us -> 29.5 us
    pallas_call x0 -> x4, Pallas kernels: none -> 146 us  [the longest x1 54.2 us: gather_experts(): pl.pallas_call(gather_body, out_shape=[part, part], in_specs=[hbm, vmem,...]
    dot_general x39 -> x5, matrix products: 85.9 us -> 7.18 us  [the longest x1 2.73 us: body(): jnp.dot(heads, w_out, preferred_element_type=jnp.float32)]
    all_gather x2 -> x1, waiting for transfers between devices: 65 us -> 0.01 us  [body(): pairs = lax.all_gather(key_pairs, 'ep', axis=0, tiled=True)]
    reduce_sum x19 -> x3, other arithmetic: 52.5 us -> 2.5 us  [the longest x1 2.36 us: body(): jnp.sum(route_weights[:, :, None] * picked.astype(jnp.float32), axis=1)]
    all_to_all x3 -> x0, waiting for transfers between devices: 35.8 us -> none  [the longest x1 22.1 us: mixer_half(): lax.all_to_all(packed, 'tp', split_axis=2, concat_axis=0, tiled=True)]
    all_to_all x3 -> x0, starting transfers between devices: 22.4 us -> none  [the longest x1 10.4 us: mixer_half(): lax.all_to_all(packed, 'tp', split_axis=2, concat_axis=0, tiled=True)]
    all_to_all x1 -> x0, blocking collectives: 18.7 us -> none  [expert_half(): lax.all_to_all(outgoing, 'ep', split_axis=0, concat_axis=0, tiled=True)]
    squeeze x16 -> x0, local copies, waits for them, and re-layouts: 15.6 us -> none  [attend(): return lax.scan(step_block, fold_state, blocks)[0]]
  transfers between devices with their start and end apart: 6 -> 1, of which waited for: 5 -> 0; matrix products, arithmetic and copies ran while one was open for 49% -> 2% of each run, Pallas kernels for 0% -> 26%
where the time goes in v1:
time: 211 us; the launch traced here: 210 us
  Pallas kernels  146 us (69%)
  local copies, waits for them, and re-layouts  29.5 us (14%)
  between operations  14.5 us (7%)
  other arithmetic  13.1 us (6%)
  matrix products  7.18 us (3%)
    pallas_call x1, Pallas kernels, gather_experts(): pl.pallas_call(gather_body, out_shape=[part, part], in_specs=[hbm, vmem,...  54.2 us
    pallas_call x1, Pallas kernels, scatter_experts(): pl.pallas_call(functools.partial(scatter_body, query_tile, key_block), ou...  52.8 us
    pallas_call x2, Pallas kernels, exchange(): pl.pallas_call(exchange_body, out_shape=[jax.ShapeDtypeStruct(a.shape, a....  38.6 us
    unnamed x34, local copies, waits for them, and re-layouts  8.62 us
    convert_element_type x3, local copies, waits for them, and re-layouts, normalize(): widened = values.astype(jnp.float32)  5.96 us
  transfers between devices with their start and end apart: 1, of which 0 were waited for; matrix products, arithmetic and copies ran while one was open for 2% of the time, Pallas kernels for 26%

profile of v1, /device:TPU:1, one launch (start us, length us, event | category | flops | bytes accessed | tf_op | source)
XLA Modules:
  0.0 209.9 jit_solution(12613354152825818013)
XLA Ops:
  7.2 0.9 copy.97
  9.6 1.3 compare_and_fusion
  10.9 1.1 fusion.1
  12.0 1.3 convolution_convert_fusion
  13.8 1.3 convolution_convert_fusion.4
  15.2 1.3 convolution_convert_fusion.3
  18.0 23.5 %exchange.2 = (bf16[16,144,128]{2,1,0:T(8,128)(2,1)S(1)}, bf16[16,96,128]{2,1,0:T(8,128)(2,1)S(1)}) custom-call(bf16[16,144,128]{2,1,0:T(8,128)(2,1)S(1)} %reshape.412.x_ref, bf16[16,96,128]{2,1,0:T(8,128)(2,1)S(1)} %pad_maximum_fusion.y_ref), custom_call_target="tpu_custom_call" | custom-call | flops 10000000000 | bytes 1000000 | tf_op jit(solution)/shard_map/exchange/pallas_call | solution.py:95
  43.6 0.9 copy.107
  44.5 1.3 reshape.430
  45.8 1.4 copy.103
  47.2 3.3 %reshape.429 = f32[1024,2,2,16]{0,3,2,1:T(8,128)} reshape(f32[16,2,32,64]{2,1,0,3:T(2,128)} %bitcast.56) | data formatting | bytes 524288 | tf_op jit(solution)/shard_map/convert_element_type | solution.py:22
  50.5 1.3 mul.212
  51.7 1.3 reduce_sum.75
  53.0 1.1 copy.104
  54.4 1.0 multiply_multiply_fusion
  55.5 1.6 fusion.27
  57.2 0.9 pad_maximum_fusion.1
  58.5 1.3 reshape.420
  59.8 1.9 copy.109
  63.4 1.2 copy-done.1
  64.6 1.2 copy-done.2
  65.8 1.3 copy-done.3
  67.1 54.2 %gather_experts.1 = (bf16[16,144,1024]{2,1,0:T(8,128)(2,1)S(1)}, bf16[16,144,1024]{2,1,0:T(8,128)(2,1)}) custom-call(bf16[2,144,1024]{2,1,0:T(8,128)(2,1)S(1)} %copy.110.rows_ref, bf16[2,1024,256]{2,1,0:T(8,128)(2,1)S(1)} %copy-done.1, bf16[2,1024,256]{2,1,0:T(8,128)(2,1)S(1)} %copy-done.2, bf16[2,256,1024]{2,1,0:T(8,128)(2,1)S(1)} %copy-done.3), custom_call_target="tpu_custom_call" | custom-call | flops 49999998976 | bytes 20000000 | tf_op jit(solution)/shard_map/gather_experts/pallas_call | solution.py:253
  121.3 2.2 %copy-done.6 = bf16[16,144,1024]{2,1,0:T(8,128)(2,1)} copy-done((bf16[16,144,1024]{2,1,0:T(8,128)(2,1)}, bf16[16,144,1024]{2,1,0:T(8,128)(2,1)S(1)}, u32[]{:S(2)}) %copy-start.6) | copy-done | bytes 4718616
  123.4 52.8 %scatter_experts.1 = (bf16[2,144,1024]{2,1,0:T(8,128)(2,1)S(1)}, bf16[1024,128]{1,0:T(8,128)(2,1)S(1)}) custom-call(bf16[1024,128]{1,0:T(8,128)(2,1)S(1)} %pad.4.query_ref, bf16[16384,128]{1,0:T(8,128)(2,1)} %all-gather.2.cloned.1.call-done.pair_ref, bf16[16,144,1024]{2,1,0:T(8,128)(2,1)} %copy-done.6, bf16[16,144,1024]{2,1,0:T(8,128)(2,1)} %get-tuple-element.13.part_hbm), custom_call_target="tpu_custom_call" | custom-call | flops 49999998976 | bytes 20000000 | tf_op jit(solution)/shard_map/scatter_experts/pallas_call | solution.py:401
  177.0 1.2 copy.112
  178.2 1.5 reshape.423.x_ref
  179.7 0.9 copy-done.5
  180.6 15.0 %exchange.3 = (bf16[16,144,128]{2,1,0:T(8,128)(2,1)S(1)}, bf16[16,64,128]{2,1,0:T(8,128)(2,1)S(1)}) custom-call(bf16[16,144,128]{2,1,0:T(8,128)(2,1)S(1)} %reshape.423.x_ref, bf16[16,64,128]{2,1,0:T(8,128)(2,1)S(1)} %bitcast.55), custom_call_target="tpu_custom_call" | custom-call | flops 10000000000 | bytes 1000000 | tf_op jit(solution)/shard_map/exchange/pallas_call | solution.py:95
  195.9 1.3 gather_fusion
  197.9 2.7 %fusion = bf16[64,1,1024]{2,0,1:T(8,128)(2,1)} fusion(bf16[64,1024]{1,0:T(8,128)(2,1)S(1)} %reshape.425, bf16[1024,1024]{1,0:T(8,128)(2,1)} %param.22), kind=kOutput, calls=%fused_computation.4 | convolution fusion | flops 134283264 | bytes 2359296 | tf_op jit(solution)/shard_map/dot_general | solution.py:516
  200.7 2.4 %multiply_reduce_fusion = bf16[128,1024]{1,0:T(8,128)(2,1)} fusion(bf16[128,2,1024]{2,1,0:T(2,128)(2,1)S(1)} %gather.7, pred[128,2]{1,0:T(8,128)(4,1)S(1)} %copy.115, f32[128,2]{1,0:T(8,128)S(1)} %copy-done.8), kind=kLoop, calls=%fused_computation.7 | loop fusion | flops 917504 | bytes 787712 | tf_op jit(solution)/shard_map/reduce_sum | solution.py:519
  (86 shorter events, 9.6 us)
Async XLA Ops:
  7.2 9.6 %copy-start = (bf16[1024,1024]{1,0:T(8,128)(2,1)S(1)}, bf16[1024,1024]{1,0:T(8,128)(2,1)}, u32[]{:S(2)}) copy-start(bf16[1024,1024]{1,0:T(8,128)(2,1)} %param.17) | copy-start | bytes 6291460
  7.2 6.4 %copy-start.7 = (bf16[64,1,1024]{2,0,1:T(8,128)(2,1)S(1)}, bf16[64,1,1024]{2,0,1:T(8,128)(2,1)}, u32[]{:S(2)}) copy-start(bf16[64,1,1024]{2,0,1:T(8,128)(2,1)} %param.15) | copy-start | bytes 393220
  7.2 6.6 %copy-start.9 = (f32[1024]{0:T(1024)S(1)}, f32[1024]{0:T(1024)}, u32[]{:S(2)}) copy-start(f32[1024]{0:T(1024)} %param.16) | copy-start | bytes 12292
  7.2 116.2 %all-gather.2.cloned.1.call-start = ((), (), s32[]{:S(2)}) async-start(), calls=%async_computation | async-start | bytes 4456448 | tf_op jit(solution)/shard_map/all_gather | solution.py:503
  9.4 2.6 %copy-start.10 = (s32[256]{0:T(256)}, s32[256]{0:T(256)S(1)}, u32[]{:S(2)}) copy-start(s32[256]{0:T(256)S(1)} %fusion.32) | copy-start | bytes 3076
  41.5 1.9 copy-start.15
  45.8 8.5 %copy-start.14 = (f32[64]{0:T(128)S(1)}, f32[64]{0:T(128)}, u32[]{:S(2)}) copy-start(f32[64]{0:T(128)} %param.20) | copy-start | bytes 772
  58.5 3.3 %copy-start.12 = (pred[128,2]{0,1:T(4,128)(4,1)S(1)}, pred[128,2]{0,1:T(4,128)(4,1)}, u32[]{:S(2)}) copy-start(pred[128,2]{0,1:T(4,128)(4,1)} %get-tuple-element.18) | copy-start | bytes 772
  58.5 3.5 %copy-start.13 = (f32[128,2]{0,1:T(2,128)S(1)}, f32[128,2]{0,1:T(2,128)}, u32[]{:S(2)}) copy-start(f32[128,2]{0,1:T(2,128)} %param.26) | copy-start | bytes 3076
  59.8 3.0 %copy-start.11 = (s32[256]{0:T(256)S(1)}, s32[256]{0:T(256)}, u32[]{:S(2)}) copy-start(s32[256]{0:T(256)} %copy-done.10) | copy-start | bytes 3076
  63.4 1.2 copy-start.1
  64.6 1.2 copy-start.2
  65.8 1.3 copy-start.3
  121.3 2.2 %copy-start.6 = (bf16[16,144,1024]{2,1,0:T(8,128)(2,1)}, bf16[16,144,1024]{2,1,0:T(8,128)(2,1)S(1)}, u32[]{:S(2)}) copy-start(bf16[16,144,1024]{2,1,0:T(8,128)(2,1)S(1)} %get-tuple-element.12.own_hbm) | copy-start | bytes 14155780
  176.2 0.7 copy-start.4
  179.6 1.0 copy-start.5
  197.4 3.3 %copy-start.8 = (f32[128,2]{1,0:T(8,128)S(1)}, f32[128,2]{1,0:T(8,128)}, u32[]{:S(2)}) copy-start(f32[128,2]{1,0:T(8,128)} %copy.114) | copy-start | bytes 3076
Sparse Core Ops, SparseCore 0:
  58.2 51.9 all-gather.1

commit v2 on v1

v2 whole, which is shorter than its diff:
```python
import functools
import math

import jax
import jax.numpy as jnp
from jax import lax
from jax.experimental import pallas as pl
from jax.experimental.pallas import tpu as pltpu
from jax.sharding import PartitionSpec as P

HEAD = 64
GRID_W = 64
LANES = 128
EXP2_SCALE = HEAD ** (-0.5) * math.log2(math.e)
MESH = pl.DeviceIdType.MESH
MIB = 1024 * 1024
BF16, F32 = jnp.bfloat16, jnp.float32
VMEM_SPEC = pl.BlockSpec(memory_space=pltpu.VMEM)
HBM_SPEC = pl.BlockSpec(memory_space=pltpu.HBM)
DMA = pltpu.SemaphoreType.DMA


epsilon = 1e-06


def normalize(values, gain_vec):
    widened = values.astype(F32)
    return (
        widened
        * lax.rsqrt(jnp.mean(widened * widened, axis=-1, keepdims=True) + epsilon)
        * gain_vec
    )


def matmul(left, right):
    return jnp.dot(left, right, preferred_element_type=F32)


def angle_tables(positions, head_size):
    quarter = head_size // 4
    frequency = 10000.0 ** (-jnp.arange(quarter, dtype=F32) / quarter)
    grid_pos = jnp.stack([positions // GRID_W, positions % GRID_W], axis=-1).astype(F32)
    angles = grid_pos[:, :, None] * frequency[None, None, :]
    return (jnp.cos(angles), jnp.sin(angles))


def lane_tables(positions):
    cosine, sine = angle_tables(positions, HEAD)
    rows = cosine.shape[0]
    cosine = jnp.stack([cosine, cosine], axis=2).reshape(rows, HEAD)
    sine = jnp.stack([-sine, sine], axis=2).reshape(rows, HEAD)
    return jnp.tile(cosine, (1, LANES // HEAD)), jnp.tile(sine, (1, LANES // HEAD))


def greet(peers):
    barrier = pltpu.get_barrier_semaphore()
    for peer in peers:
        pl.semaphore_signal(barrier, inc=1, device_id=peer, device_id_type=MESH)


def await_greetings(count):
    pl.semaphore_wait(pltpu.get_barrier_semaphore(), count)


def axis_peers(axis):
    me, count = lax.axis_index(axis), lax.axis_size(axis)
    return [lax.rem(me + d, count) for d in range(count)]


def remote(source, target, send_sem, recv_sem, device_id):
    return pltpu.make_async_remote_copy(
        src_ref=source,
        dst_ref=target,
        send_sem=send_sem,
        recv_sem=recv_sem,
        device_id=device_id,
        device_id_type=MESH,
    )


def exchange_copies(axis, sources, targets, sends, recvs):
    me = lax.axis_index(axis)
    return [
        remote(source(peer), target(me), send.at[d], recv.at[d], {axis: peer})
        for d, peer in enumerate(axis_peers(axis))
        if d > 0
        for source, target, send, recv in zip(sources, targets, sends, recvs)
    ]


def iota(shape, axis):
    return lax.broadcasted_iota(jnp.int32, shape, axis)


def slot_rows(id_rows, experts, capacity):
    choices, tokens = id_rows.shape
    marks = [
        (iota((experts, tokens), 0) == id_rows[k : k + 1, :]).astype(F32) for k in range(choices)
    ]
    earlier = (iota((tokens, tokens), 0) < iota((tokens, tokens), 1)).astype(BF16)
    ranks = matmul(functools.reduce(jnp.add, marks).astype(BF16), earlier)
    main, last = [], []
    for k in range(choices):
        rank = jnp.sum(marks[k] * ranks, axis=0, keepdims=True).astype(jnp.int32)
        ids = id_rows[k : k + 1, :]
        main.append(jnp.where(rank < capacity - 1, ids * (capacity - 1) + rank, -1))
        last.append(jnp.where(rank == capacity - 1, ids, -1))
    return main, last


def pick(rows, columns, first, stride):
    wanted = iota((rows, columns), 0) * stride + first
    return (iota((rows, columns), 1) == wanted).astype(BF16)


def place(rows, columns, first, stride):
    wanted = iota((rows, columns), 1) * stride + first
    return (iota((rows, columns), 0) == wanted).astype(BF16)


def head_turner(cosine, sine, pair_sums):
    lane = iota(cosine.shape, 1)
    quarter = HEAD // 4

    def turned(raw, gain):
        values = raw.astype(BF16).astype(F32)
        squares = values * values
        high = squares.astype(BF16)
        low = (squares - high.astype(F32)).astype(BF16)
        sums = matmul(high, pair_sums) + matmul(low, pair_sums)
        values = values * lax.rsqrt(sums * (1.0 / HEAD) + epsilon) * gain
        partner = jnp.where(
            lax.rem(lane, 2 * quarter) < quarter,
            pltpu.roll(values, LANES - quarter, 1),
            pltpu.roll(values, quarter, 1),
        )
        return (values * cosine + partner * sine).astype(BF16).astype(F32)

    return turned


def dispatch_body(
    mix_ref,
    mix_gain_ref,
    query_hbm,
    key_hbm,
    value_hbm,
    query_gain_ref,
    key_gain_ref,
    cosine_ref,
    sine_ref,
    token_ref,
    token_gain_ref,
    ids_ref,
    head_out,
    main_out,
    last_out,
    w_query,
    w_key,
    w_value,
    head_send,
    main_send,
    last_send,
    last_recv,
    load_sem,
    head_sems,
    main_sems,
    last_sems,
):
    tp_count, ep_count = lax.axis_size("tp"), lax.axis_size("ep")
    tp_me, ep_me = lax.axis_index("tp"), lax.axis_index("ep")
    width = mix_ref.shape[1]
    column_tiles = width // LANES
    local_experts, capacity = main_out.shape[0], main_out.shape[2] + 1
    experts = local_experts * ep_count
    greet([{"tp": p} for p in axis_peers("tp")[1:]] + [{"ep": p} for p in axis_peers("ep")[1:]])
    loads = [
        pltpu.make_async_copy(hbm, vmem, load_sem.at[i])
        for i, (hbm, vmem) in enumerate(
            ((query_hbm, w_query), (key_hbm, w_key), (value_hbm, w_value))
        )
    ]
    for load in loads:
        load.start()

    normed = normalize(token_ref[...], token_gain_ref[...]).astype(BF16)
    main, last = slot_rows(ids_ref[...], experts, capacity)
    tokens = normed.shape[0]
    main_rows, last_rows = experts * (capacity - 1), experts * column_tiles
    slots = iota((main_rows, tokens), 0)
    hits = functools.reduce(jnp.add, [(slots == row).astype(F32) for row in main])
    main_send[...] = (
        matmul(hits.astype(BF16), normed).astype(BF16).reshape(main_send.shape)
    )
    slots = iota((last_rows, tokens), 0)
    tiles = jnp.zeros((last_rows, LANES), F32)
    for c in range(column_tiles):
        hits = [
            (slots == jnp.where(row >= 0, row * column_tiles + c, -1)).astype(F32) for row in last
        ]
        hits = functools.reduce(jnp.add, hits).astype(BF16)
        tiles = tiles + matmul(hits, normed[:, c * LANES : (c + 1) * LANES])
    last_send[...] = tiles.astype(BF16).reshape(last_send.shape)
    await_greetings(tp_count + ep_count - 2)
    copies = exchange_copies(
        "ep",
        (lambda e: main_send.at[e], lambda e: last_send.at[e]),
        (lambda e: main_out.at[:, e], lambda e: last_recv.at[e]),
        (main_sems.at[0], last_sems.at[0]),
        (main_sems.at[1], last_sems.at[1]),
    )
    for copy in copies:
        copy.start()

    normed = normalize(mix_ref[...], mix_gain_ref[...]).astype(BF16)
    rows = normed.shape[0]
    half = rows // 2
    pair_sums = iota((LANES, LANES), 0) // HEAD == iota((LANES, LANES), 1) // HEAD
    turned = head_turner(cosine_ref[...], sine_ref[...], pair_sums.astype(BF16))
    query_gain = jnp.concatenate([query_gain_ref[...]] * (LANES // HEAD), axis=1)
    key_gain = jnp.concatenate([key_gain_ref[...]] * (LANES // HEAD), axis=1)
    lower = iota((rows, LANES), 1) < HEAD
    lower_half = iota((half, LANES), 1) < HEAD
    for load in loads:
        load.wait()
    keys, values = matmul(normed, w_key[...]), matmul(normed, w_value[...])
    key_heads = w_key.shape[1] // HEAD
    group = tp_count // key_heads
    for t in range(key_heads // 2):
        key = turned(keys[:, t * LANES : (t + 1) * LANES], key_gain)
        value = values[:, t * LANES : (t + 1) * LANES].astype(BF16).astype(F32)
        for h, pairs in enumerate(
            (
                jnp.where(lower, key, pltpu.roll(value, HEAD, 1)),
                jnp.where(lower, pltpu.roll(key, HEAD, 1), value),
            )
        ):
            pairs = pairs.astype(BF16)
            for member in range(group):
                part = member % 2 * half
                head_send[(2 * t + h) * group + member, :half, :] = pairs[part : part + half]
    queries = matmul(normed, w_query[...])
    for t in range(tp_count // 2):
        tile = turned(queries[:, t * LANES : (t + 1) * LANES], query_gain)
        first, second = tile[:half], tile[half:]
        head_send[2 * t, half:, :] = jnp.where(
            lower_half, first, pltpu.roll(second, HEAD, 1)
        ).astype(BF16)
        head_send[2 * t + 1, half:, :] = jnp.where(
            lower_half, pltpu.roll(first, HEAD, 1), second
        ).astype(BF16)
    head_copies = exchange_copies(
        "tp",
        (lambda t: head_send.at[t],),
        (lambda t: head_out.at[t],),
        (head_sems.at[0],),
        (head_sems.at[1],),
    )
    for copy in head_copies:
        copy.start()

    head_out[tp_me] = head_send[tp_me]
    last_recv[ep_me] = last_send[ep_me]
    for j in range(local_experts):
        main_out[j, ep_me] = main_send[ep_me, j]
    for copy in copies:
        copy.wait()
    tiles = last_recv[...].reshape(last_rows, LANES)
    for j in range(local_experts):
        for c in range(column_tiles):
            chosen = pick(ep_count, last_rows, j * column_tiles + c, local_experts * column_tiles)
            last_out[j, :, c * LANES : (c + 1) * LANES] = matmul(chosen, tiles).astype(BF16)
    for copy in head_copies:
        copy.wait()


def dispatch(
    mix, mix_gain, w_query, w_key, w_value, query_gain, key_gain, cosine, sine, tokens, gain, ids,
    local_experts, capacity,
):
    tp_count, ep_count = lax.axis_size("tp"), lax.axis_size("ep")
    rows, width = mix.shape
    main = (capacity - 1, width)
    last = (ep_count, local_experts * width // LANES, LANES)
    head = (tp_count, rows, LANES)
    return pl.pallas_call(
        dispatch_body,
        out_shape=[
            jax.ShapeDtypeStruct(head, BF16),
            jax.ShapeDtypeStruct((local_experts, ep_count) + main, BF16),
            jax.ShapeDtypeStruct((local_experts, ep_count, width), BF16),
        ],
        in_specs=[VMEM_SPEC] * 2 + [HBM_SPEC] * 3 + [VMEM_SPEC] * 7,
        out_specs=[VMEM_SPEC] * 3,
        scratch_shapes=[
            pltpu.VMEM(w_query.shape, BF16),
            pltpu.VMEM(w_key.shape, BF16),
            pltpu.VMEM(w_value.shape, BF16),
            pltpu.VMEM(head, BF16),
            pltpu.VMEM((ep_count, local_experts) + main, BF16),
            pltpu.VMEM(last, BF16),
            pltpu.VMEM(last, BF16),
            DMA((3,)),
            DMA((2, tp_count)),
            DMA((2, ep_count)),
            DMA((2, ep_count)),
        ],
        name="dispatch",
        compiler_params=pltpu.CompilerParams(
            collective_id=0, has_side_effects=True, vmem_limit_bytes=63 * MIB
        ),
    )(mix, mix_gain, w_query, w_key, w_value, query_gain, key_gain, cosine, sine, tokens, gain, ids)


def ring_places():
    me = lax.axis_index("tp")
    chips = lax.axis_size("tp") // 2
    chip, core = me // 2, lax.rem(me, 2)
    ahead = lax.rem(chip + 1 - 2 * core + chips, chips) * 2 + core
    behind = lax.rem(chip - 1 + 2 * core + chips, chips) * 2 + core
    partner = chip * 2 + 1 - core
    return core, {"tp": ahead}, {"tp": behind}, {"tp": partner}


def gather_body(
    head_ref,
    main_ref,
    last_ref,
    gate_hbm,
    up_hbm,
    down_hbm,
    own_out,
    pair_out,
    keys_out,
    gate,
    up,
    down,
    held,
    own_part,
    pair_part,
    load_sem,
    key_sem,
    ring_sems,
    pair_sems,
    own_sem,
    part_sems,
    key_sems,
    share_sems,
):
    pieces, _, piece_rows, width = held.shape
    core, ahead, behind, partner = ring_places()
    ep_me, ep_count = lax.axis_index("ep"), lax.axis_size("ep")
    greet([ahead, behind, partner] + [{"ep": p} for p in axis_peers("ep")[1:]])
    loads = [
        pltpu.make_async_copy(hbm, vmem, load_sem.at[i])
        for i, (hbm, vmem) in enumerate(((gate_hbm, gate), (up_hbm, up), (down_hbm, down)))
    ]
    for load in loads:
        load.start()
    tail_rows = last_ref.shape[1]
    for j in range(2):
        held[j, 0, : piece_rows - tail_rows, :] = main_ref[j].reshape(
            piece_rows - tail_rows, width
        )
        held[j, 0, piece_rows - tail_rows :, :] = last_ref[j]

    def ring_copy(i):
        return remote(
            held.at[i, 0], held.at[i + 2, 0], ring_sems.at[0, i], ring_sems.at[1, i], ahead
        )

    def pair_copy(i):
        return remote(
            held.at[i, 0], held.at[i, 1], pair_sems.at[0, i], pair_sems.at[1, i], partner
        )

    def part_copy(i):
        return remote(
            pair_part.at[i], pair_out.at[i], part_sems.at[0, i], part_sems.at[1, i], partner
        )

    def own_copy(i):
        return pltpu.make_async_copy(own_part.at[i], own_out.at[i], own_sem.at[i])

    half = head_ref.shape[1] // 2
    own_keys = head_ref.at[:, pl.ds(0, half), :]
    key_copies = exchange_copies(
        "ep",
        (lambda e: own_keys,),
        (lambda e: keys_out.at[core, e],),
        (key_sems.at[0],),
        (key_sems.at[1],),
    )
    keep_keys = pltpu.make_async_copy(own_keys, keys_out.at[core, ep_me], key_sem.at[0])

    def share(source, d):
        origin = lax.rem(ep_me - d + ep_count, ep_count)
        target = keys_out.at[core, origin]
        return remote(
            target if source is None else source,
            target,
            share_sems.at[0, d],
            share_sems.at[1, d],
            partner,
        )

    def key_arrival(d):
        target = keys_out.at[core, lax.rem(ep_me - d + ep_count, ep_count)]
        return remote(target, target, key_sems.at[0, d], key_sems.at[1, d], partner)

    await_greetings(ep_count + 2)

    def step(i, _):
        @pl.when(i < pieces)
        def _():
            @pl.when(i >= 2)
            def _():
                ring_copy(i - 2).wait_recv()

            @pl.when(i < pieces - 2)
            def _():
                ring_copy(i).start()

            pair_copy(i).start()

        @pl.when(i == 1)
        def _():
            for copy in key_copies:
                copy.start()
            keep_keys.start()
            share(own_keys, 0).start()
            for load in loads:
                load.wait()

        @pl.when(i >= 3)
        def _():
            key_arrival(i - 2).wait_recv()
            share(None, i - 2).start()

        @pl.when(jnp.logical_and(i >= 1, i <= pieces))
        def _():
            piece = i - 1
            expert = lax.rem(piece, 2)
            pair_copy(piece).wait_recv()
            rows = held[piece].reshape(2 * piece_rows, width)
            gate_act = matmul(rows, gate[expert])
            up_act = matmul(rows, up[expert])
            hidden = (gate_act / (1.0 + jnp.exp(-gate_act)) * up_act).astype(BF16)
            sums = matmul(hidden, down[expert]).astype(BF16)
            own_part[piece] = sums[:piece_rows]
            pair_part[piece] = sums[piece_rows:]

        @pl.when(i >= 2)
        def _():
            own_copy(i - 2).start()
            part_copy(i - 2).start()

        return 0

    lax.fori_loop(0, pieces + 2, step, 0)

    def finish(i, _):
        @pl.when(i < pieces - 2)
        def _():
            ring_copy(i).wait_send()

        pair_copy(i).wait_send()
        own_copy(i).wait()
        part_copy(i).wait()
        return 0

    lax.fori_loop(0, pieces, finish, 0)
    keep_keys.wait()
    for copy in key_copies:
        copy.wait_send()

    def finish_share(d, _):
        share(None, d).wait()
        return 0

    lax.fori_loop(0, ep_count, finish_share, 0)


def gather_experts(head, main, last, w_gate, w_up, w_down):
    pieces, ep_count = lax.axis_size("tp"), lax.axis_size("ep")
    piece_rows, width = ep_count * (main.shape[2] + 1), main.shape[3]
    part = (pieces, piece_rows, width)
    keys = (2, ep_count, pieces, head.shape[1] // 2, LANES)
    assert pieces == ep_count
    return pl.pallas_call(
        gather_body,
        out_shape=[jax.ShapeDtypeStruct(shape, BF16) for shape in (part, part, keys)],
        in_specs=[VMEM_SPEC] * 3 + [HBM_SPEC] * 3,
        out_specs=[HBM_SPEC] * 3,
        scratch_shapes=[
            pltpu.VMEM(w_gate.shape, BF16),
            pltpu.VMEM(w_up.shape, BF16),
            pltpu.VMEM(w_down.shape, BF16),
            pltpu.VMEM((pieces, 2, piece_rows, width), BF16),
            pltpu.VMEM(part, BF16),
            pltpu.VMEM(part, BF16),
            DMA((3,)),
            DMA((1,)),
            DMA((2, pieces)),
            DMA((2, pieces)),
            DMA((pieces,)),
            DMA((2, pieces)),
            DMA((2, ep_count)),
            DMA((2, ep_count)),
        ],
        name="gather_experts",
        compiler_params=pltpu.CompilerParams(
            collective_id=1, has_side_effects=True, vmem_limit_bytes=63 * MIB
        ),
    )(head, main, last, w_gate, w_up, w_down)


def scatter_body(
    query_tile,
    key_block,
    head_ref,
    keys_hbm,
    own_hbm,
    part_hbm,
    main_out,
    last_out,
    mixed_out,
    queries,
    pairs,
    own_part,
    pair_part,
    arrived,
    leaving,
    row_max,
    row_sum,
    row_acc,
    key_sem,
    own_sem,
    part_sem,
    ring_sems,
):
    pieces, piece_rows, width = own_part.shape
    groups, rows, _ = head_ref.shape
    half = rows // 2
    tiles, blocks = groups * rows // query_tile, pairs.shape[0] // key_block
    slices = tiles * blocks // pieces
    tile_groups = query_tile // rows
    main_rows = piece_rows - last_out.shape[1]
    _, ahead, behind, _ = ring_places()
    greet([ahead, behind])

    def loads(i):
        slot = lax.rem(i + 2, pieces)
        return (
            pltpu.make_async_copy(own_hbm.at[slot], own_part.at[i], own_sem.at[i]),
            pltpu.make_async_copy(part_hbm.at[slot], pair_part.at[i], part_sem.at[i]),
        )

    def key_load(block):
        chosen = pl.ds(pl.multiple_of(block * key_block, key_block), key_block)
        return pltpu.make_async_copy(keys_hbm.at[chosen, :], pairs.at[chosen, :], key_sem.at[block])

    def ring_copy(i):
        return remote(leaving.at[i], arrived.at[i], ring_sems.at[0, i], ring_sems.at[1, i], ahead)

    def start_loads(i, _):
        for load in loads(i):
            load.start()

        @pl.when(i < blocks)
        def _():
            key_load(i).start()

        return 0

    lax.fori_loop(0, pieces, start_loads, 0)
    packed = head_ref[:, half:, :].astype(F32).reshape(groups * half, LANES)
    lower = iota(packed.shape, 1) < HEAD
    for h, values in enumerate((packed, pltpu.roll(packed, HEAD, 1))):
        values = jnp.where(lower, values, 0.0).astype(BF16).reshape(groups, half, LANES)
        queries[:, h * half : (h + 1) * half, :] = values
    row_max[...] = jnp.full(row_max.shape, -1e30, F32)
    row_sum[...] = jnp.zeros(row_sum.shape, F32)
    row_acc[...] = jnp.zeros(row_acc.shape, F32)
    await_greetings(2)

    def attend_slice(number):
        block, tile = number // tiles, lax.rem(number, tiles)
        chosen = queries[pl.ds(tile * tile_groups, tile_groups)].reshape(query_tile, LANES)
        keys = pairs[pl.ds(pl.multiple_of(block * key_block, key_block), key_block), :]
        scores = lax.dot_general(
            chosen, keys, (((1,), (1,)), ((), ())), preferred_element_type=F32
        )
        old_max = row_max[tile][:, :1]
        new_max = jnp.maximum(old_max, jnp.max(scores, axis=1, keepdims=True))
        shrink = jnp.exp2((old_max - new_max) * EXP2_SCALE)
        raised = jnp.exp2((scores - new_max) * EXP2_SCALE)
        lane_sums = raised[:, :LANES]
        for lane in range(LANES, key_block, LANES):
            lane_sums = lane_sums + raised[:, lane : lane + LANES]
        row_max[tile] = jnp.broadcast_to(new_max, (query_tile, LANES))
        row_sum[tile] = row_sum[tile] * shrink + lane_sums
        row_acc[tile] = row_acc[tile] * shrink + matmul(raised.astype(BF16), keys)

    def step(i, _):
        for load in loads(i):
            load.wait()

        @pl.when(i < 2)
        def _():
            total = own_part[i].astype(F32) + pair_part[i].astype(F32)
            leaving[i] = total.astype(BF16)

        @pl.when(i >= 2)
        def _():
            ring_copy(i - 2).wait_recv()
            total = own_part[i].astype(F32) + pair_part[i].astype(F32)
            total = (total + arrived[i - 2].astype(F32)).astype(BF16)

            @pl.when(i < pieces - 2)
            def _():
                leaving[i] = total

            @pl.when(i >= pieces - 2)
            def _():
                j = i - (pieces - 2)
                main_out[j] = total[:main_rows].reshape(main_out.shape[1:])
                last_out[j] = total[main_rows:]

        @pl.when(i < pieces - 2)
        def _():
            ring_copy(i).start()

        @pl.when(lax.rem(i * slices, tiles) == 0)
        def _():
            key_load(i * slices // tiles).wait()

        for part in range(slices):
            attend_slice(i * slices + part)
        return 0

    lax.fori_loop(0, pieces, step, 0)

    def finish(i, _):
        ring_copy(i).wait_send()
        return 0

    lax.fori_loop(0, pieces - 2, finish, 0)
    for tile in range(tiles):
        mixed = row_acc[tile] / jnp.sum(row_sum[tile], axis=1, keepdims=True)
        mixed_out[tile * tile_groups : (tile + 1) * tile_groups] = mixed.astype(BF16).reshape(
            tile_groups, rows, LANES
        )


def scatter_experts(head, keys, own_part, pair_part, capacity):
    pieces, piece_rows, width = own_part.shape
    groups, rows, _ = head.shape
    key_count = keys.shape[0]
    query_tile, key_block = math.gcd(groups * rows, 256), math.gcd(key_count, 2048)
    tiles = groups * rows // query_tile
    ep_count = piece_rows // capacity
    state = pltpu.VMEM((tiles, query_tile, LANES), F32)
    return pl.pallas_call(
        functools.partial(scatter_body, query_tile, key_block),
        out_shape=[
            jax.ShapeDtypeStruct((2, ep_count, capacity - 1, width), BF16),
            jax.ShapeDtypeStruct((2, ep_count, width), BF16),
            jax.ShapeDtypeStruct(head.shape, BF16),
        ],
        in_specs=[VMEM_SPEC] + [HBM_SPEC] * 3,
        out_specs=[VMEM_SPEC] * 3,
        scratch_shapes=[
            pltpu.VMEM(head.shape, BF16),
            pltpu.VMEM(keys.shape, BF16),
            pltpu.VMEM((pieces, piece_rows, width), BF16),
            pltpu.VMEM((pieces, piece_rows, width), BF16),
            pltpu.VMEM((pieces - 2, piece_rows, width), BF16),
            pltpu.VMEM((pieces - 2, piece_rows, width), BF16),
            state,
            state,
            state,
            DMA((key_count // key_block,)),
            DMA((pieces,)),
            DMA((pieces,)),
            DMA((2, pieces - 2)),
        ],
        name="scatter_experts",
        compiler_params=pltpu.CompilerParams(
            collective_id=2, has_side_effects=True, vmem_limit_bytes=63 * MIB
        ),
    )(head, keys, own_part, pair_part)


def collect_body(
    main_ref,
    last_ref,
    mixed_ref,
    out_hbm,
    ids_ref,
    weights_ref,
    mix_out,
    experts_out,
    w_out,
    results,
    last_send,
    last_recv,
    main_recv,
    mixed_recv,
    load_sem,
    head_sems,
    main_sems,
    last_sems,
):
    tp_count, ep_count = lax.axis_size("tp"), lax.axis_size("ep")
    tp_me, ep_me = lax.axis_index("tp"), lax.axis_index("ep")
    local_experts, _, main_cap, width = main_ref.shape
    column_tiles = width // LANES
    experts = local_experts * ep_count
    main_rows, last_rows = experts * main_cap, experts * column_tiles
    greet([{"tp": p} for p in axis_peers("tp")[1:]] + [{"ep": p} for p in axis_peers("ep")[1:]])
    load = pltpu.make_async_copy(out_hbm, w_out, load_sem.at[0])
    load.start()
    tiles = jnp.zeros((last_rows, LANES), F32)
    for j in range(local_experts):
        for c in range(column_tiles):
            spot = place(last_rows, ep_count, j * column_tiles + c, local_experts * column_tiles)
            tiles = tiles + matmul(spot, last_ref[j, :, c * LANES : (c + 1) * LANES])
    last_send[...] = tiles.astype(BF16).reshape(last_send.shape)
    await_greetings(tp_count + ep_count - 2)
    copies = exchange_copies(
        "ep",
        (lambda e: main_ref.at[:, e], lambda e: last_send.at[e]),
        (lambda e: main_recv.at[e], lambda e: last_recv.at[e]),
        (main_sems.at[0], last_sems.at[0]),
        (main_sems.at[1], last_sems.at[1]),
    )
    head_copies = exchange_copies(
        "tp",
        (lambda t: mixed_ref.at[t],),
        (lambda t: mixed_recv.at[t],),
        (head_sems.at[0],),
        (head_sems.at[1],),
    )
    for copy in head_copies + copies:
        copy.start()
    mixed_recv[tp_me] = mixed_ref[tp_me]
    last_recv[ep_me] = last_send[ep_me]
    for j in range(local_experts):
        main_recv[ep_me, j] = main_ref[j, ep_me]

    main, last = slot_rows(ids_ref[...], experts, main_cap + 1)
    tokens = ids_ref.shape[1]
    takers = []
    for k in range(len(main)):
        slot = jnp.where(main[k] >= 0, main[k], jnp.where(last[k] >= 0, last[k] + main_rows, -1))
        spot = (iota((results.shape[0], tokens), 0) == slot).astype(F32)
        takers.append(jnp.transpose(spot).astype(BF16))
    load.wait()
    for copy in head_copies:
        copy.wait()
    lower = iota((mixed_recv.shape[1], LANES), 1) < HEAD
    heads = []
    for t in range(tp_count // 2):
        even, odd = mixed_recv[2 * t].astype(F32), mixed_recv[2 * t + 1].astype(F32)
        heads.append(jnp.where(lower, pltpu.roll(even, HEAD, 1), odd).astype(BF16))
    mix_out[...] = matmul(jnp.concatenate(heads, axis=1), w_out[...]).astype(BF16)

    for copy in copies:
        copy.wait()
    results[:main_rows, :] = main_recv[...].reshape(main_rows, width)
    results[main_rows:, :] = jnp.zeros((results.shape[0] - main_rows, width), BF16)
    tiles = last_recv[...].reshape(last_rows, LANES)
    for c in range(column_tiles):
        chosen = matmul(pick(experts, last_rows, c, column_tiles), tiles)
        results[main_rows : main_rows + experts, c * LANES : (c + 1) * LANES] = chosen.astype(BF16)
    combined = jnp.zeros((tokens, width), F32)
    for k, taker in enumerate(takers):
        combined = combined + weights_ref[:, k : k + 1] * matmul(taker, results[...])
    experts_out[...] = combined.astype(BF16)


def collect(main, last, mixed, w_out, ids, weights):
    tp_count, ep_count = lax.axis_size("tp"), lax.axis_size("ep")
    local_experts, _, main_cap, width = main.shape
    experts = local_experts * ep_count
    result_rows = -(-experts * (main_cap + 1) // LANES) * LANES
    tiles = (ep_count, local_experts * width // LANES, LANES)
    return pl.pallas_call(
        collect_body,
        out_shape=[
            jax.ShapeDtypeStruct((mixed.shape[1], w_out.shape[1]), BF16),
            jax.ShapeDtypeStruct((ids.shape[1], width), BF16),
        ],
        in_specs=[VMEM_SPEC] * 3 + [HBM_SPEC] + [VMEM_SPEC] * 2,
        out_specs=[VMEM_SPEC] * 2,
        scratch_shapes=[
            pltpu.VMEM(w_out.shape, BF16),
            pltpu.VMEM((result_rows, width), BF16),
            pltpu.VMEM(tiles, BF16),
            pltpu.VMEM(tiles, BF16),
            pltpu.VMEM((ep_count, local_experts, main_cap, width), BF16),
            pltpu.VMEM(mixed.shape, BF16),
            DMA((1,)),
            DMA((2, tp_count)),
            DMA((2, ep_count)),
            DMA((2, ep_count)),
        ],
        name="collect",
        compiler_params=pltpu.CompilerParams(
            collective_id=3, has_side_effects=True, vmem_limit_bytes=63 * MIB
        ),
    )(main, last, mixed, w_out, ids, weights)


def body(
    mix_tokens,
    mix_gain,
    w_query,
    w_key,
    w_value,
    query_gain,
    key_gain,
    w_out,
    expert_tokens,
    expert_gain,
    route_ids,
    route_weights,
    w_gate,
    w_up,
    w_down,
):
    tp_count, ep_count = lax.axis_size("tp"), lax.axis_size("ep")
    seq_rows, _, model_width = mix_tokens.shape
    tok_count, top_count = route_ids.shape
    local_experts = w_gate.shape[0]
    capacity = tok_count * top_count * 9 // (8 * local_experts * ep_count)
    first = (lax.axis_index("ep") * tp_count + lax.axis_index("tp")) * seq_rows
    cosine, sine = lane_tables(first + jnp.arange(seq_rows, dtype=jnp.int32))
    id_rows = jnp.transpose(route_ids)
    head, main, last = dispatch(
        mix_tokens.reshape(seq_rows, model_width),
        mix_gain.reshape(1, model_width),
        w_query,
        w_key,
        w_value,
        query_gain.reshape(1, HEAD),
        key_gain.reshape(1, HEAD),
        cosine,
        sine,
        expert_tokens,
        expert_gain.reshape(1, model_width),
        id_rows,
        local_experts,
        capacity,
    )
    own_part, pair_part, keys = gather_experts(head, main, last, w_gate, w_up, w_down)
    keys = keys.reshape(-1, LANES)
    main, last, mixed = scatter_experts(head, keys, own_part, pair_part, capacity)
    mix_out, experts_out = collect(main, last, mixed, w_out, id_rows, route_weights)
    return (mix_out[:, None, :], experts_out)


def solution(mesh):
    placed = (
        P(("ep", "tp"), None, None),
        P(),
        P(),
        P(),
        P(),
        P(),
        P(),
        P(),
        P(("ep", "tp"), None),
        P(),
        P(("ep", "tp"), None),
        P(("ep", "tp"), None),
        P("ep", None, "tp"),
        P("ep", None, "tp"),
        P("ep", "tp", None),
    )
    return jax.shard_map(
        body,
        mesh=mesh,
        in_specs=placed,
        out_specs=(P(("ep", "tp"), None, None), P(("ep", "tp"), None)),
        check_vma=False,
    )
```

time: 211 us -> 161 us (0.76)
  local copies, waits for them, and re-layouts: 29.5 us -> 5.63 us
  between operations: 14.5 us -> 0.73 us
  other arithmetic: 13.1 us -> 0.19 us
  Pallas kernels: 146 us -> 155 us
  matrix products: 7.18 us -> 0 us
    pallas_call x3, Pallas kernels: 92.7 us -> 103 us  [the longest x1 59.9 us: gather_experts(): pl.pallas_call(gather_body, out_shape=[jax.ShapeDtypeStruct(shape, BF16)...]
    dot_general x5 -> x0, matrix products: 7.18 us -> none  [the longest x1 2.73 us: body(): jnp.dot(heads, w_out, preferred_element_type=jnp.float32)]
    convert_element_type x5 -> x0, local copies, waits for them, and re-layouts: 6.3 us -> none  [the longest x3 5.96 us: normalize(): widened = values.astype(jnp.float32)]
    reduce_sum x7 -> x0, other arithmetic: 5.23 us -> none  [the longest x4 2.73 us: normalize(): jnp.mean(widened * widened, axis=-1, keepdims=True) + epsilon]
    unnamed x34 -> x5, local copies, waits for them, and re-layouts: 8.62 us -> 3.98 us
    reshape x12 -> x0, local copies, waits for them, and re-layouts: 4.53 us -> none  [the longest x1 1.47 us: body(): jnp.transpose(summed, (1, 0, 2, 3)).reshape(ep_count, lane_rows, 128)]
    transpose x5 -> x0, local copies, waits for them, and re-layouts: 3.41 us -> none  [the longest x1 1.88 us: body(): jnp.transpose(rows, (1, 0, 2, 3))]
    mul x3 -> x0, local copies, waits for them, and re-layouts: 2.24 us -> none  [the longest x1 1.27 us: normalize(): widened * widened]
  transfers between devices with their start and end apart: 1 -> 0, of which waited for: 0 -> 0; matrix products, arithmetic and copies ran while one was open for 2% -> 0% of each run, Pallas kernels for 26% -> 0%
where the time goes in v2:
time: 161 us
  Pallas kernels  155 us (96%)
  local copies, waits for them, and re-layouts  5.63 us (3%)
    pallas_call x1, Pallas kernels, gather_experts(): pl.pallas_call(gather_body, out_shape=[jax.ShapeDtypeStruct(shape, BF16)...  59.9 us
    pallas_call x1, Pallas kernels, scatter_experts(): pl.pallas_call(functools.partial(scatter_body, query_tile, key_block), ou...  52.1 us
    pallas_call x1, Pallas kernels, dispatch(): pl.pallas_call(dispatch_body, out_shape=[jax.ShapeDtypeStruct(head, BF16)...  24.1 us
    pallas_call x1, Pallas kernels, collect(): pl.pallas_call(collect_body, out_shape=[jax.ShapeDtypeStruct((mixed.shape...  18.5 us
    unnamed x5, local copies, waits for them, and re-layouts  3.98 us

profile of v2, /device:TPU:1, one launch (start us, length us, event | category | flops | bytes accessed | tf_op | source)
XLA Modules:
  0.0 161.2 jit_solution(933209450906431352)
XLA Ops:
  0.7 0.1 fusion
  0.8 0.1 copy.19
  1.0 0.7 tile.25.sine_ref
  1.7 0.1 copy.18
  1.8 0.7 tile.22.cosine_ref
  2.5 24.1 %dispatch.1 = (bf16[16,64,128]{2,1,0:T(8,128)(2,1)}, bf16[2,16,8,1024]{3,2,1,0:T(8,128)(2,1)}, bf16[2,16,1024]{2,1,0:T(8,128)(2,1)}) custom-call(bf16[64,1024]{1,0:T(8,128)(2,1)} %bitcast.11, f32[1,1024]{1,0:T(1,128)} %bitcast.15, bf16[1024,1024]{1,0:T(8,128)(2,1)} %query_hbm.1, bf16[1024,256]{1,0:T(8,128)(2,1)} %key_hbm.1, bf16[1024,256]{1,0:T(8,128)(2,1)} %value_hbm.1, ...), custom_call_target="tpu_custom_call" | custom-call | tf_op jit(solution)/shard_map/dispatch/pallas_call | solution.py:286
  26.7 59.9 %gather_experts.1 = (bf16[16,144,1024]{2,1,0:T(8,128)(2,1)}, bf16[16,144,1024]{2,1,0:T(8,128)(2,1)}, bf16[2,16,16,32,128]{4,3,2,1,0:T(8,128)(2,1)}) custom-call(bf16[16,64,128]{2,1,0:T(8,128)(2,1)} %get-tuple-element.13.head_ref, bf16[2,16,8,1024]{3,2,1,0:T(8,128)(2,1)} %get-tuple-element.14.main_ref, bf16[2,16,1024]{2,1,0:T(8,128)(2,1)} %get-tuple-element.15.last_ref, ...), custom_call_target="tpu_custom_call" | custom-call | tf_op jit(solution)/shard_map/gather_experts/pallas_call | solution.py:490
  86.5 0.0 copy-start
  86.6 52.1 %scatter_experts.1 = (bf16[2,16,8,1024]{3,2,1,0:T(8,128)(2,1)}, bf16[2,16,1024]{2,1,0:T(8,128)(2,1)}, bf16[16,64,128]{2,1,0:T(8,128)(2,1)}) custom-call(bf16[16,64,128]{2,1,0:T(8,128)(2,1)} %get-tuple-element.13.head_ref, bf16[16384,128]{1,0:T(8,128)(2,1)} %bitcast.10, bf16[16,144,1024]{2,1,0:T(8,128)(2,1)} %get-tuple-element.17.own_hbm, ...), custom_call_target="tpu_custom_call" | custom-call | tf_op jit(solution)/shard_map/scatter_experts/pallas_call | solution.py:664
  138.7 0.0 copy-done
  138.7 0.7 copy.20.weights_ref
  139.5 18.5 %collect.1 = (bf16[64,1024]{1,0:T(8,128)(2,1)}, bf16[128,1024]{1,0:T(8,128)(2,1)}) custom-call(bf16[2,16,8,1024]{3,2,1,0:T(8,128)(2,1)} %get-tuple-element.19.main_ref, bf16[2,16,1024]{2,1,0:T(8,128)(2,1)} %get-tuple-element.20.last_ref, bf16[16,64,128]{2,1,0:T(8,128)(2,1)} %get-tuple-element.21.mixed_ref, bf16[1024,1024]{1,0:T(8,128)(2,1)} %out_hbm.1, ...), custom_call_target="tpu_custom_call" | custom-call | tf_op jit(solution)/shard_map/collect/pallas_call | solution.py:789
  158.0 1.6 copy.23
  159.5 1.7 %copy.24 = bf16[128,1024]{1,0:T(8,128)(2,1)} copy(bf16[128,1024]{1,0:T(8,128)(2,1)} %get-tuple-element.32) | data formatting | bytes 524288
  (7 shorter events, 0.1 us)
Async XLA Ops:
  86.5 52.2 %copy-start = (f32[128,2]{0,1:T(2,128)S(1)}, f32[128,2]{0,1:T(2,128)}, u32[]{:S(2)}) copy-start(f32[128,2]{0,1:T(2,128)} %param.26) | copy-start | bytes 3076

commit v3 on v0

v3 whole, which is shorter than its diff:
```python
import functools
import math

import jax
import jax.numpy as jnp
from jax import lax
from jax.experimental import pallas as pl
from jax.experimental.pallas import tpu as pltpu
import numpy as np
from jax.sharding import PartitionSpec as P

HEAD = 64
GRID_W = 64
LANES = 128
KEY_GROUPS = 4
EXP2_SCALE = HEAD ** (-0.5) * math.log2(math.e)
MESH = pl.DeviceIdType.MESH
MIB = 1024 * 1024
BF16, F32 = jnp.bfloat16, jnp.float32
VMEM_SPEC = pl.BlockSpec(memory_space=pltpu.VMEM)
HBM_SPEC = pl.BlockSpec(memory_space=pltpu.HBM)
DMA = pltpu.SemaphoreType.DMA


epsilon = 1e-06


def normalize(values, gain_vec):
    widened = values.astype(F32)
    return (
        widened
        * lax.rsqrt(jnp.mean(widened * widened, axis=-1, keepdims=True) + epsilon)
        * gain_vec
    )


def matmul(left, right):
    return jnp.dot(left, right, preferred_element_type=F32)


def frequencies():
    quarter = HEAD // 4
    powers = np.float32(10000.0) ** (-np.arange(quarter, dtype=np.float32) / np.float32(quarter))
    return np.tile(powers.astype(np.float32), LANES // quarter).reshape(1, LANES)


def greet(peers):
    barrier = pltpu.get_barrier_semaphore()
    for peer in peers:
        pl.semaphore_signal(barrier, inc=1, device_id=peer, device_id_type=MESH)


def await_greetings(count):
    pl.semaphore_wait(pltpu.get_barrier_semaphore(), count)


def axis_peers(axis):
    me, count = lax.axis_index(axis), lax.axis_size(axis)
    return [lax.rem(me + d, count) for d in range(count)]


def remote(source, target, send_sem, recv_sem, device_id):
    return pltpu.make_async_remote_copy(
        src_ref=source,
        dst_ref=target,
        send_sem=send_sem,
        recv_sem=recv_sem,
        device_id=device_id,
        device_id_type=MESH,
    )


def exchange_copies(axis, sources, targets, sends, recvs):
    me = lax.axis_index(axis)
    return [
        remote(source(peer), target(me), send.at[d], recv.at[d], {axis: peer})
        for d, peer in enumerate(axis_peers(axis))
        if d > 0
        for source, target, send, recv in zip(sources, targets, sends, recvs)
    ]


def iota(shape, axis):
    return lax.broadcasted_iota(jnp.int32, shape, axis)


def slot_rows(id_rows, experts, capacity):
    choices, tokens = id_rows.shape
    marks = [
        (iota((experts, tokens), 0) == id_rows[k : k + 1, :]).astype(F32) for k in range(choices)
    ]
    earlier = (iota((tokens, tokens), 0) < iota((tokens, tokens), 1)).astype(BF16)
    ranks = matmul(functools.reduce(jnp.add, marks).astype(BF16), earlier)
    main, last = [], []
    for k in range(choices):
        rank = jnp.sum(marks[k] * ranks, axis=0, keepdims=True).astype(jnp.int32)
        ids = id_rows[k : k + 1, :]
        main.append(jnp.where(rank < capacity - 1, ids * (capacity - 1) + rank, -1))
        last.append(jnp.where(rank == capacity - 1, ids, -1))
    return main, last


def pick(rows, columns, first, stride):
    wanted = iota((rows, columns), 0) * stride + first
    return (iota((rows, columns), 1) == wanted).astype(BF16)


def place(rows, columns, first, stride):
    wanted = iota((rows, columns), 1) * stride + first
    return (iota((rows, columns), 0) == wanted).astype(BF16)


def head_turner(first, rows, powers, pair_sums):
    lane = iota((rows, LANES), 1)
    quarter = HEAD // 4
    position = first + iota((rows, LANES), 0)
    by_row = lax.rem(lane, HEAD) < HEAD // 2
    place = jnp.where(by_row, position // GRID_W, lax.rem(position, GRID_W)).astype(F32)
    angles = place * powers
    cosine = jnp.cos(angles)
    sine = jnp.sin(angles)
    sine = jnp.where(lax.rem(lane, 2 * quarter) < quarter, -sine, sine)

    def turned(raw, gain):
        values = raw.astype(BF16).astype(F32)
        squares = values * values
        high = squares.astype(BF16)
        low = (squares - high.astype(F32)).astype(BF16)
        sums = matmul(high, pair_sums) + matmul(low, pair_sums)
        values = values * lax.rsqrt(sums * (1.0 / HEAD) + epsilon) * gain
        partner = jnp.where(
            lax.rem(lane, 2 * quarter) < quarter,
            pltpu.roll(values, LANES - quarter, 1),
            pltpu.roll(values, quarter, 1),
        )
        return (values * cosine + partner * sine).astype(BF16).astype(F32)

    return turned


def ring_places():
    me = lax.axis_index("tp")
    chips = lax.axis_size("tp") // 2
    chip, core = me // 2, lax.rem(me, 2)
    ahead = lax.rem(chip + 1 - 2 * core + chips, chips) * 2 + core
    behind = lax.rem(chip - 1 + 2 * core + chips, chips) * 2 + core
    partner = chip * 2 + 1 - core
    return core, {"tp": ahead}, {"tp": behind}, {"tp": partner}


def layer_body(
    mix_ref,
    mix_gain_ref,
    query_hbm,
    key_hbm,
    value_hbm,
    query_gain_ref,
    key_gain_ref,
    powers_ref,
    out_hbm,
    token_ref,
    token_gain_ref,
    ids_ref,
    weights_ref,
    gate_hbm,
    up_hbm,
    down_hbm,
    mix_out,
    experts_out,
    w_query,
    w_key,
    w_value,
    w_out,
    gate,
    up,
    down,
    head_send,
    head_recv,
    main_send,
    main_in,
    last_send,
    last_in,
    held,
    own_part,
    pair_part,
    pair_in,
    leaving,
    arrived,
    keys,
    queries,
    row_max,
    row_sum,
    row_acc,
    mixed_send,
    mixed_recv,
    main_back,
    main_recv,
    last_back,
    last_recv,
    results,
    load_sem,
    head_sems,
    main_sems,
    last_sems,
    ring_sems,
    pair_sems,
    part_sems,
    sum_sems,
    key_sems,
    share_sems,
    mixed_sems,
    main_back_sems,
    last_back_sems,
):
    tp_count, ep_count = lax.axis_size("tp"), lax.axis_size("ep")
    tp_me, ep_me = lax.axis_index("tp"), lax.axis_index("ep")
    core, ahead, behind, partner = ring_places()
    greet([{"tp": p} for p in axis_peers("tp")[1:]] + [{"ep": p} for p in axis_peers("ep")[1:]])
    loads = [
        pltpu.make_async_copy(hbm, vmem, load_sem.at[i])
        for i, (hbm, vmem) in enumerate(
            (
                (query_hbm, w_query),
                (key_hbm, w_key),
                (value_hbm, w_value),
                (gate_hbm, gate),
                (up_hbm, up),
                (down_hbm, down),
                (out_hbm, w_out),
            )
        )
    ]
    for load in loads:
        load.start()

    local_experts, _, main_cap, width = main_in.shape
    column_tiles = width // LANES
    experts = local_experts * ep_count
    capacity = main_cap + 1
    tokens = token_ref.shape[0]
    main_rows, last_rows = experts * main_cap, experts * column_tiles
    normed = normalize(token_ref[...], token_gain_ref[...]).astype(BF16)
    main, last = slot_rows(ids_ref[...], experts, capacity)
    slots = iota((main_rows, tokens), 0)
    hits = functools.reduce(jnp.add, [(slots == row).astype(F32) for row in main])
    main_send[...] = matmul(hits.astype(BF16), normed).astype(BF16).reshape(main_send.shape)
    slots = iota((last_rows, tokens), 0)
    tiles = jnp.zeros((last_rows, LANES), F32)
    for c in range(column_tiles):
        hits = [
            (slots == jnp.where(row >= 0, row * column_tiles + c, -1)).astype(F32) for row in last
        ]
        hits = functools.reduce(jnp.add, hits).astype(BF16)
        tiles = tiles + matmul(hits, normed[:, c * LANES : (c + 1) * LANES])
    last_send[...] = tiles.astype(BF16).reshape(last_send.shape)
    await_greetings(tp_count + ep_count - 2)
    row_copies = exchange_copies(
        "ep",
        (lambda e: main_send.at[e], lambda e: last_send.at[e]),
        (lambda e: main_in.at[:, e], lambda e: last_in.at[e]),
        (main_sems.at[0], last_sems.at[0]),
        (main_sems.at[1], last_sems.at[1]),
    )
    for copy in row_copies:
        copy.start()

    normed = normalize(mix_ref[...], mix_gain_ref[...]).astype(BF16)
    rows = normed.shape[0]
    half = rows // 2
    pair_sums = iota((LANES, LANES), 0) // HEAD == iota((LANES, LANES), 1) // HEAD
    turned = head_turner(
        (ep_me * tp_count + tp_me) * rows, rows, powers_ref[...], pair_sums.astype(BF16)
    )
    query_gain = jnp.concatenate([query_gain_ref[...]] * (LANES // HEAD), axis=1)
    key_gain = jnp.concatenate([key_gain_ref[...]] * (LANES // HEAD), axis=1)
    lower = iota((rows, LANES), 1) < HEAD
    lower_half = iota((half, LANES), 1) < HEAD
    for load in loads[:3]:
        load.wait()
    raw_keys, raw_values = matmul(normed, w_key[...]), matmul(normed, w_value[...])
    key_heads = w_key.shape[1] // HEAD
    group = tp_count // key_heads
    for t in range(key_heads // 2):
        key = turned(raw_keys[:, t * LANES : (t + 1) * LANES], key_gain)
        value = raw_values[:, t * LANES : (t + 1) * LANES].astype(BF16).astype(F32)
        for h, pairs in enumerate(
            (
                jnp.where(lower, key, pltpu.roll(value, HEAD, 1)),
                jnp.where(lower, pltpu.roll(key, HEAD, 1), value),
            )
        ):
            pairs = pairs.astype(BF16)
            for member in range(group):
                part = member % 2 * half
                head_send[(2 * t + h) * group + member, :half, :] = pairs[part : part + half]
    raw_queries = matmul(normed, w_query[...])
    for t in range(tp_count // 2):
        tile = turned(raw_queries[:, t * LANES : (t + 1) * LANES], query_gain)
        first, second = tile[:half], tile[half:]
        head_send[2 * t, half:, :] = jnp.where(
            lower_half, first, pltpu.roll(second, HEAD, 1)
        ).astype(BF16)
        head_send[2 * t + 1, half:, :] = jnp.where(
            lower_half, pltpu.roll(first, HEAD, 1), second
        ).astype(BF16)
    head_copies = exchange_copies(
        "tp",
        (lambda t: head_send.at[t],),
        (lambda t: head_recv.at[t],),
        (head_sems.at[0],),
        (head_sems.at[1],),
    )
    for copy in head_copies:
        copy.start()
    head_recv[tp_me] = head_send[tp_me]
    last_in[ep_me] = last_send[ep_me]
    for j in range(local_experts):
        main_in[j, ep_me] = main_send[ep_me, j]
    row_max[...] = jnp.full(row_max.shape, -1e30, F32)
    row_sum[...] = jnp.zeros(row_sum.shape, F32)
    row_acc[...] = jnp.zeros(row_acc.shape, F32)

    pieces, _, piece_rows, _ = held.shape
    held_main = ep_count * main_cap
    for copy in row_copies:
        copy.wait_recv()
    tiles = last_in[...].reshape(last_rows, LANES)
    for j in range(local_experts):
        held[j, 0, :held_main, :] = main_in[j].reshape(held_main, width)
        for c in range(column_tiles):
            chosen = pick(ep_count, last_rows, j * column_tiles + c, local_experts * column_tiles)
            held[j, 0, held_main:, c * LANES : (c + 1) * LANES] = matmul(chosen, tiles).astype(BF16)
    def ring_copy(i):
        return remote(
            held.at[i, 0], held.at[i + 2, 0], ring_sems.at[0, i], ring_sems.at[1, i], ahead
        )

    def pair_copy(i):
        return remote(
            held.at[i, 0], held.at[i, 1], pair_sems.at[0, i], pair_sems.at[1, i], partner
        )

    def part_copy(i):
        return remote(
            pair_part.at[i], pair_in.at[i], part_sems.at[0, i], part_sems.at[1, i], partner
        )

    def sum_copy(m):
        return remote(leaving.at[m], arrived.at[m], sum_sems.at[0, m], sum_sems.at[1, m], ahead)

    own_keys = head_recv.at[:, pl.ds(0, half), :]
    key_copies = [
        remote(
            own_keys, keys.at[core, d], key_sems.at[0, d], key_sems.at[1, d], {"ep": peer}
        )
        for d, peer in enumerate(axis_peers("ep"))
        if d > 0
    ]

    def key_arrival(d):
        return remote(
            keys.at[core, d], keys.at[core, d], key_sems.at[0, d], key_sems.at[1, d], partner
        )

    def share(d):
        return remote(
            keys.at[core, d], keys.at[core, d], share_sems.at[0, d], share_sems.at[1, d], partner
        )

    tiles_count, tile_rows, _ = row_acc.shape
    tile_groups = tile_rows // rows
    groups = tp_count
    key_group = ep_count // KEY_GROUPS
    key_rows = key_group * groups * half

    def attend_slice(tile, block):
        chosen = queries[tile * tile_groups : (tile + 1) * tile_groups].reshape(tile_rows, LANES)
        pairs = keys[lax.rem(block, 2), pl.ds(block // 2 * key_group, key_group)]
        pairs = pairs.reshape(key_rows, LANES)
        scores = lax.dot_general(
            chosen, pairs, (((1,), (1,)), ((), ())), preferred_element_type=F32
        )
        old_max = row_max[tile][:, :1]
        new_max = jnp.maximum(old_max, jnp.max(scores, axis=1, keepdims=True))
        shrink = jnp.exp2((old_max - new_max) * EXP2_SCALE)
        raised = jnp.exp2((scores - new_max) * EXP2_SCALE)
        lane_sums = raised[:, :LANES]
        for lane in range(LANES, key_rows, LANES):
            lane_sums = lane_sums + raised[:, lane : lane + LANES]
        row_max[tile] = jnp.broadcast_to(new_max, (tile_rows, LANES))
        row_sum[tile] = row_sum[tile] * shrink + lane_sums
        row_acc[tile] = row_acc[tile] * shrink + matmul(raised.astype(BF16), pairs)

    def step(i, _):
        @pl.when(jnp.logical_and(i >= 2, i < pieces + 2))
        def _():
            part_copy(i - 2).start()

        @pl.when(i < pieces)
        def _():
            @pl.when(i >= 2)
            def _():
                ring_copy(i - 2).wait_recv()

            @pl.when(i < pieces - 2)
            def _():
                ring_copy(i).start()

            pair_copy(i).start()

        @pl.when(i == 1)
        def _():
            for load in loads[3:]:
                load.wait()

        @pl.when(i == 2)
        def _():
            for copy in head_copies:
                copy.wait_recv()
            for copy in key_copies:
                copy.start()
            keys[core, 0] = head_recv[:, :half, :]
            packed = head_recv[:, half:, :].astype(F32).reshape(groups * half, LANES)
            lower_lanes = iota(packed.shape, 1) < HEAD
            for h, values in enumerate((packed, pltpu.roll(packed, HEAD, 1))):
                values = jnp.where(lower_lanes, values, 0.0).astype(BF16)
                queries[:, h * half : (h + 1) * half, :] = values.reshape(groups, half, LANES)

        @pl.when(jnp.logical_and(i >= 4, i < 4 + KEY_GROUPS))
        def _():
            for g in range(key_group):
                d = (i - 4) * key_group + g

                @pl.when(d > 0)
                def _():
                    key_arrival(d).wait_recv()

                share(d).start()

        @pl.when(jnp.logical_and(i >= 1, i <= pieces))
        def _():
            piece = i - 1
            expert = lax.rem(piece, 2)
            pair_copy(piece).wait_recv()
            values = held[piece].reshape(2 * piece_rows, width)
            gate_act = matmul(values, gate[expert])
            up_act = matmul(values, up[expert])
            hidden = (gate_act / (1.0 + jnp.exp(-gate_act)) * up_act).astype(BF16)
            sums = matmul(hidden, down[expert]).astype(BF16)
            own_part[piece] = sums[:piece_rows]
            pair_part[piece] = sums[piece_rows:]

        @pl.when(jnp.logical_and(i >= 6, i < 6 + 2 * KEY_GROUPS))
        def _():
            block = i - 6

            @pl.when(lax.rem(block, 2) == 0)
            def _():
                for g in range(key_group):
                    share(block // 2 * key_group + g).wait_recv()

            for tile in range(tiles_count):
                attend_slice(tile, block)

        @pl.when(i >= 4)
        def _():
            m = i - 4
            piece = lax.rem(m + 2, pieces)
            part_copy(piece).wait_recv()

            @pl.when(m < 2)
            def _():
                total = own_part[piece].astype(F32) + pair_in[piece].astype(F32)
                leaving[m] = total.astype(BF16)

            @pl.when(m >= 2)
            def _():
                sum_copy(m - 2).wait_recv()
                total = own_part[piece].astype(F32) + pair_in[piece].astype(F32)
                total = (total + arrived[m - 2].astype(F32)).astype(BF16)

                @pl.when(m < pieces - 2)
                def _():
                    leaving[m] = total

                @pl.when(m >= pieces - 2)
                def _():
                    j = m - (pieces - 2)
                    main_back[j] = total[:held_main].reshape(main_back.shape[1:])
                    last_back[j] = total[held_main:]

            @pl.when(m < pieces - 2)
            def _():
                sum_copy(m).start()

        @pl.when(i == pieces)
        def _():
            for tile in range(tiles_count):
                mixed = row_acc[tile] / jnp.sum(row_sum[tile], axis=1, keepdims=True)
                mixed_send[tile * tile_groups : (tile + 1) * tile_groups] = mixed.astype(
                    BF16
                ).reshape(tile_groups, rows, LANES)

        return 0

    lax.fori_loop(0, pieces + 4, step, 0)
    for copy in row_copies + head_copies:
        copy.wait_send()

    tiles = jnp.zeros((last_rows, LANES), F32)
    for j in range(local_experts):
        for c in range(column_tiles):
            spot = place(last_rows, ep_count, j * column_tiles + c, local_experts * column_tiles)
            tiles = tiles + matmul(spot, last_back[j, :, c * LANES : (c + 1) * LANES])
    last_send[...] = tiles.astype(BF16).reshape(last_send.shape)
    back_copies = exchange_copies(
        "ep",
        (lambda e: main_back.at[:, e], lambda e: last_send.at[e]),
        (lambda e: main_recv.at[e], lambda e: last_recv.at[e]),
        (main_back_sems.at[0], last_back_sems.at[0]),
        (main_back_sems.at[1], last_back_sems.at[1]),
    )
    mixed_copies = exchange_copies(
        "tp",
        (lambda t: mixed_send.at[t],),
        (lambda t: mixed_recv.at[t],),
        (mixed_sems.at[0],),
        (mixed_sems.at[1],),
    )
    for copy in back_copies + mixed_copies:
        copy.start()
    mixed_recv[tp_me] = mixed_send[tp_me]
    last_recv[ep_me] = last_send[ep_me]
    for j in range(local_experts):
        main_recv[ep_me, j] = main_back[j, ep_me]

    def finish(i, _):
        @pl.when(i < pieces - 2)
        def _():
            ring_copy(i).wait_send()
            sum_copy(i).wait_send()

        pair_copy(i).wait_send()
        part_copy(i).wait_send()
        return 0

    lax.fori_loop(0, pieces, finish, 0)
    for copy in key_copies:
        copy.wait_send()

    def finish_share(d, _):
        share(d).wait_send()
        return 0

    lax.fori_loop(0, ep_count, finish_share, 0)

    main, last = slot_rows(ids_ref[...], experts, capacity)
    takers = []
    for k in range(len(main)):
        slot = jnp.where(main[k] >= 0, main[k], jnp.where(last[k] >= 0, last[k] + main_rows, -1))
        spot = (iota((results.shape[0], tokens), 0) == slot).astype(F32)
        takers.append(jnp.transpose(spot).astype(BF16))
    results[main_rows:, :] = jnp.zeros((results.shape[0] - main_rows, width), BF16)
    for copy in mixed_copies:
        copy.wait()
    heads = []
    for t in range(tp_count // 2):
        even, odd = mixed_recv[2 * t].astype(F32), mixed_recv[2 * t + 1].astype(F32)
        heads.append(jnp.where(lower, pltpu.roll(even, HEAD, 1), odd).astype(BF16))
    mix_out[...] = matmul(jnp.concatenate(heads, axis=1), w_out[...]).astype(BF16)

    for copy in back_copies:
        copy.wait()
    results[:main_rows, :] = main_recv[...].reshape(main_rows, width)
    tiles = last_recv[...].reshape(last_rows, LANES)
    for c in range(column_tiles):
        chosen = matmul(pick(experts, last_rows, c, column_tiles), tiles)
        results[main_rows : main_rows + experts, c * LANES : (c + 1) * LANES] = chosen.astype(BF16)
    combined = jnp.zeros((tokens, width), F32)
    for k, taker in enumerate(takers):
        row = jnp.broadcast_to(weights_ref[k : k + 1, :], (tokens, tokens))
        combined = combined + jnp.transpose(row)[:, :1] * matmul(taker, results[...])
    experts_out[...] = combined.astype(BF16)


def layer(
    mix, mix_gain, w_query, w_key, w_value, query_gain, key_gain, powers, w_out, tokens, gain, ids,
    weights, w_gate, w_up, w_down, capacity,
):
    pieces, ep_count = lax.axis_size("tp"), lax.axis_size("ep")
    rows, width = mix.shape
    local_experts = w_gate.shape[0]
    piece = (ep_count * capacity, width)
    head = pltpu.VMEM((pieces, rows, LANES), BF16)
    query_tile = math.gcd(pieces * rows, 256)
    state = pltpu.VMEM((pieces * rows // query_tile, query_tile, LANES), F32)
    by_device = pltpu.VMEM((ep_count, local_experts, capacity - 1, width), BF16)
    by_expert = pltpu.VMEM((local_experts, ep_count, capacity - 1, width), BF16)
    last = pltpu.VMEM((ep_count, local_experts * width // LANES, LANES), BF16)
    sums = pltpu.VMEM((pieces,) + piece, BF16)
    flights = pltpu.VMEM((pieces - 2,) + piece, BF16)
    result_rows = -(-local_experts * ep_count * capacity // LANES) * LANES
    return pl.pallas_call(
        layer_body,
        out_shape=[
            jax.ShapeDtypeStruct((rows, w_out.shape[1]), BF16),
            jax.ShapeDtypeStruct(tokens.shape, BF16),
        ],
        in_specs=[VMEM_SPEC] * 2
        + [HBM_SPEC] * 3
        + [VMEM_SPEC] * 3
        + [HBM_SPEC]
        + [VMEM_SPEC] * 4
        + [HBM_SPEC] * 3,
        out_specs=[VMEM_SPEC] * 2,
        scratch_shapes=[
            pltpu.VMEM(w.shape, BF16) for w in (w_query, w_key, w_value, w_out, w_gate, w_up, w_down)
        ]
        + [head, head, by_device, by_expert, last, last]
        + [pltpu.VMEM((pieces, 2) + piece, BF16), sums, sums, sums, flights, flights]
        + [pltpu.VMEM((2, ep_count, pieces, rows // 2, LANES), BF16), head, state, state, state]
        + [head, head, by_expert, by_device]
        + [pltpu.VMEM((local_experts, ep_count, width), BF16), last]
        + [pltpu.VMEM((result_rows, width), BF16)]
        + [DMA((7,)), DMA((2, pieces)), DMA((2, ep_count)), DMA((2, ep_count))]
        + [DMA((2, pieces))] * 4
        + [DMA((2, ep_count))] * 2
        + [DMA((2, pieces)), DMA((2, ep_count)), DMA((2, ep_count))],
        name="layer",
        compiler_params=pltpu.CompilerParams(
            collective_id=0, has_side_effects=True, vmem_limit_bytes=62 * MIB
        ),
    )(
        mix, mix_gain, w_query, w_key, w_value, query_gain, key_gain, powers, w_out, tokens, gain,
        ids, weights, w_gate, w_up, w_down,
    )


def body(
    mix_tokens,
    mix_gain,
    w_query,
    w_key,
    w_value,
    query_gain,
    key_gain,
    w_out,
    expert_tokens,
    expert_gain,
    route_ids,
    route_weights,
    w_gate,
    w_up,
    w_down,
):
    ep_count = lax.axis_size("ep")
    seq_rows, _, model_width = mix_tokens.shape
    tok_count, top_count = route_ids.shape
    local_experts = w_gate.shape[0]
    capacity = tok_count * top_count * 9 // (8 * local_experts * ep_count)
    id_rows = jnp.transpose(route_ids)
    mix_out, experts_out = layer(
        mix_tokens.reshape(seq_rows, model_width),
        mix_gain.reshape(1, model_width),
        w_query,
        w_key,
        w_value,
        query_gain.reshape(1, HEAD),
        key_gain.reshape(1, HEAD),
        frequencies(),
        w_out,
        expert_tokens,
        expert_gain.reshape(1, model_width),
        id_rows,
        jnp.transpose(route_weights),
        w_gate,
        w_up,
        w_down,
        capacity,
    )
    return (mix_out[:, None, :], experts_out)


def solution(mesh):
    placed = (
        P(("ep", "tp"), None, None),
        P(),
        P(),
        P(),
        P(),
        P(),
        P(),
        P(),
        P(("ep", "tp"), None),
        P(),
        P(("ep", "tp"), None),
        P(("ep", "tp"), None),
        P("ep", None, "tp"),
        P("ep", None, "tp"),
        P("ep", "tp", None),
    )
    return jax.shard_map(
        body,
        mesh=mesh,
        in_specs=placed,
        out_specs=(P(("ep", "tp"), None, None), P(("ep", "tp"), None)),
        check_vma=False,
    )
```

time: 341 us -> 139 us (0.41)
  Pallas kernels: 0 us -> 134 us
  waiting for transfers between devices: 101 us -> 0 us
  matrix products: 85.9 us -> 0 us
  other arithmetic: 61.8 us -> 0 us
  local copies, waits for them, and re-layouts: 35 us -> 3.24 us
  starting transfers between devices: 22.7 us -> 0 us
  blocking collectives: 18.7 us -> 0 us
  between operations: 14.2 us -> 0.64 us
    pallas_call x0 -> x1, Pallas kernels: none -> 134 us  [layer(): pl.pallas_call(layer_body, out_shape=[jax.ShapeDtypeStruct((rows, w_out.s...]
    dot_general x39 -> x0, matrix products: 85.9 us -> none  [the longest x16 43.4 us: step_block(): jnp.einsum('qshd,ksd->qshk', queries, keys_part, preferred_element_type=j...]
    all_gather x2 -> x0, waiting for transfers between devices: 65 us -> none  [the longest x1 36.4 us: mixer_half(): lax.all_gather(key_pairs, 'ep', axis=0, tiled=True)]
    reduce_sum x23 -> x0, other arithmetic: 54 us -> none  [the longest x16 50 us: step_block(): totals = totals * shrink + jnp.sum(raised, axis=-1)]
    all_to_all x3 -> x0, waiting for transfers between devices: 35.8 us -> none  [the longest x1 22.1 us: mixer_half(): lax.all_to_all(packed, 'tp', split_axis=2, concat_axis=0, tiled=True)]
    all_to_all x3 -> x0, starting transfers between devices: 22.4 us -> none  [the longest x1 10.4 us: mixer_half(): lax.all_to_all(packed, 'tp', split_axis=2, concat_axis=0, tiled=True)]
    all_to_all x1 -> x0, blocking collectives: 18.7 us -> none  [expert_half(): lax.all_to_all(outgoing, 'ep', split_axis=0, concat_axis=0, tiled=True)]
    squeeze x16 -> x0, local copies, waits for them, and re-layouts: 15.6 us -> none  [attend(): return lax.scan(step_block, fold_state, blocks)[0]]
  transfers between devices with their start and end apart: 6 -> 0, of which waited for: 5 -> 0; matrix products, arithmetic and copies ran while one was open for 49% -> 0% of each run, Pallas kernels for 0% -> 0%
where the time goes in v3:
time: 139 us; the launch traced here: 138 us
  Pallas kernels  134 us (96%)
  local copies, waits for them, and re-layouts  3.24 us (2%)
    pallas_call x1, Pallas kernels, layer(): pl.pallas_call(layer_body, out_shape=[jax.ShapeDtypeStruct((rows, w_out.s...  134 us
    unnamed x2, local copies, waits for them, and re-layouts  3.24 us

profile of v3, /device:TPU:1, one launch (start us, length us, event | category | flops | bytes accessed | tf_op | source)
XLA Modules:
  0.0 137.9 jit_solution(9502091348401938986)
XLA Ops:
  0.6 134.0 %layer.1 = (bf16[64,1024]{1,0:T(8,128)(2,1)}, bf16[128,1024]{1,0:T(8,128)(2,1)}) custom-call(bf16[64,1024]{1,0:T(8,128)(2,1)} %bitcast.8, f32[1,1024]{1,0:T(1,128)} %bitcast.10, bf16[1024,1024]{1,0:T(8,128)(2,1)} %query_hbm.1, bf16[1024,256]{1,0:T(8,128)(2,1)} %key_hbm.1, bf16[1024,256]{1,0:T(8,128)(2,1)} %value_hbm.1, f32[1,64]{1,0:T(1,128)} %bitcast.14, ...), custom_call_target="tpu_custom_call" | custom-call | tf_op jit(solution)/shard_map/layer/pallas_call | solution.py:603
  134.7 1.6 %copy.20 = bf16[64,1,1024]{2,0,1:T(8,128)(2,1)} copy(bf16[64,1,1024]{2,0,1:T(8,128)(2,1)} %bitcast.9) | data formatting | bytes 262144
  136.2 1.7 %copy.21 = bf16[128,1024]{1,0:T(8,128)(2,1)} copy(bf16[128,1024]{1,0:T(8,128)(2,1)} %get-tuple-element.9) | data formatting | bytes 524288

commit v4 on v3

--- a/solution.py
+++ b/solution.py
@@ -176,10 +176,8 @@
     down,
     head_send,
     head_recv,
-    main_send,
-    main_in,
-    last_send,
-    last_in,
+    rows_send,
+    rows_in,
     held,
     own_part,
     pair_part,
@@ -193,15 +191,12 @@
     row_acc,
     mixed_send,
     mixed_recv,
-    main_back,
-    main_recv,
-    last_back,
-    last_recv,
+    rows_back,
+    rows_recv,
     results,
     load_sem,
     head_sems,
-    main_sems,
-    last_sems,
+    row_sems,
     ring_sems,
     pair_sems,
     part_sems,
@@ -209,8 +204,7 @@
     key_sems,
     share_sems,
     mixed_sems,
-    main_back_sems,
-    last_back_sems,
+    back_sems,
 ):
     tp_count, ep_count = lax.axis_size("tp"), lax.axis_size("ep")
     tp_me, ep_me = lax.axis_index("tp"), lax.axis_index("ep")
@@ -233,8 +227,10 @@
     for load in loads:
         load.start()
 
-    local_experts, _, main_cap, width = main_in.shape
+    _, local_experts, _, main_cap, _ = rows_send.shape
+    width = token_ref.shape[1]
     column_tiles = width // LANES
+    tile_shape = (ep_count, local_experts, main_cap, LANES)
     experts = local_experts * ep_count
     capacity = main_cap + 1
     tokens = token_ref.shape[0]
@@ -243,7 +239,9 @@
     main, last = slot_rows(ids_ref[...], experts, capacity)
     slots = iota((main_rows, tokens), 0)
     hits = functools.reduce(jnp.add, [(slots == row).astype(F32) for row in main])
-    main_send[...] = matmul(hits.astype(BF16), normed).astype(BF16).reshape(main_send.shape)
+    outgoing = matmul(hits.astype(BF16), normed).astype(BF16)
+    for c in range(column_tiles):
+        rows_send[:, :, c] = outgoing[:, c * LANES : (c + 1) * LANES].reshape(tile_shape)
     slots = iota((last_rows, tokens), 0)
     tiles = jnp.zeros((last_rows, LANES), F32)
     for c in range(column_tiles):
@@ -252,16 +250,19 @@
         ]
         hits = functools.reduce(jnp.add, hits).astype(BF16)
         tiles = tiles + matmul(hits, normed[:, c * LANES : (c + 1) * LANES])
-    last_send[...] = tiles.astype(BF16).reshape(last_send.shape)
+    rows_send[:, :, column_tiles] = tiles.astype(BF16).reshape(tile_shape)
     await_greetings(tp_count + ep_count - 2)
-    row_copies = exchange_copies(
-        "ep",
-        (lambda e: main_send.at[e], lambda e: last_send.at[e]),
-        (lambda e: main_in.at[:, e], lambda e: last_in.at[e]),
-        (main_sems.at[0], last_sems.at[0]),
-        (main_sems.at[1], last_sems.at[1]),
-    )
-    for copy in row_copies:
+    row_copies = [
+        exchange_copies(
+            "ep",
+            (lambda e, j=j: rows_send.at[e, j],),
+            (lambda e, j=j: rows_in.at[e, j],),
+            (row_sems.at[0, j],),
+            (row_sems.at[1, j],),
+        )
+        for j in range(local_experts)
+    ]
+    for copy in row_copies[0] + row_copies[1]:
         copy.start()
 
     normed = normalize(mix_ref[...], mix_gain_ref[...]).astype(BF16)
@@ -313,23 +314,24 @@
     for copy in head_copies:
         copy.start()
     head_recv[tp_me] = head_send[tp_me]
-    last_in[ep_me] = last_send[ep_me]
-    for j in range(local_experts):
-        main_in[j, ep_me] = main_send[ep_me, j]
+    rows_in[ep_me] = rows_send[ep_me]
     row_max[...] = jnp.full(row_max.shape, -1e30, F32)
     row_sum[...] = jnp.zeros(row_sum.shape, F32)
     row_acc[...] = jnp.zeros(row_acc.shape, F32)
 
     pieces, _, piece_rows, _ = held.shape
     held_main = ep_count * main_cap
-    for copy in row_copies:
-        copy.wait_recv()
-    tiles = last_in[...].reshape(last_rows, LANES)
-    for j in range(local_experts):
-        held[j, 0, :held_main, :] = main_in[j].reshape(held_main, width)
+
+    def receive_rows(j):
+        for copy in row_copies[j]:
+            copy.wait_recv()
+        tiles = rows_in[:, j, column_tiles].reshape(ep_count * column_tiles, LANES)
         for c in range(column_tiles):
-            chosen = pick(ep_count, last_rows, j * column_tiles + c, local_experts * column_tiles)
-            held[j, 0, held_main:, c * LANES : (c + 1) * LANES] = matmul(chosen, tiles).astype(BF16)
+            columns = slice(c * LANES, (c + 1) * LANES)
+            chosen = matmul(pick(ep_count, ep_count * column_tiles, c, column_tiles), tiles)
+            held[j, 0, :held_main, columns] = rows_in[:, j, c].reshape(held_main, LANES)
+            held[j, 0, held_main:, columns] = chosen.astype(BF16)
+
     def ring_copy(i):
         return remote(
             held.at[i, 0], held.at[i + 2, 0], ring_sems.at[0, i], ring_sems.at[1, i], ahead
@@ -391,10 +393,46 @@
         row_sum[tile] = row_sum[tile] * shrink + lane_sums
         row_acc[tile] = row_acc[tile] * shrink + matmul(raised.astype(BF16), pairs)
 
+    back_copies = [
+        exchange_copies(
+            "ep",
+            (lambda e, j=j: rows_back.at[e, j],),
+            (lambda e, j=j: rows_recv.at[e, j],),
+            (back_sems.at[0, j],),
+            (back_sems.at[1, j],),
+        )
+        for j in range(local_experts)
+    ]
+    mixed_copies = exchange_copies(
+        "tp",
+        (lambda t: mixed_send.at[t],),
+        (lambda t: mixed_recv.at[t],),
+        (mixed_sems.at[0],),
+        (mixed_sems.at[1],),
+    )
+
+    def return_rows(j, total):
+        tiles = jnp.zeros((ep_count * column_tiles, LANES), F32)
+        for c in range(column_tiles):
+            columns = slice(c * LANES, (c + 1) * LANES)
+            rows_back[:, j, c] = total[:held_main, columns].reshape(ep_count, main_cap, LANES)
+            spot = place(ep_count * column_tiles, ep_count, c, column_tiles)
+            tiles = tiles + matmul(spot, total[held_main:, columns])
+        tiles = tiles.astype(BF16).reshape(ep_count, main_cap, LANES)
+        rows_back[:, j, column_tiles] = tiles
+        for copy in back_copies[j]:
+            copy.start()
+
     def step(i, _):
         @pl.when(jnp.logical_and(i >= 2, i < pieces + 2))
         def _():
             part_copy(i - 2).start()
+
+        for j in range(local_experts):
+
+            @pl.when(i == j)
+            def _(j=j):
+                receive_rows(j)
 
         @pl.when(i < pieces)
         def _():
@@ -426,10 +464,10 @@
                 values = jnp.where(lower_lanes, values, 0.0).astype(BF16)
                 queries[:, h * half : (h + 1) * half, :] = values.reshape(groups, half, LANES)
 
-        @pl.when(jnp.logical_and(i >= 4, i < 4 + KEY_GROUPS))
+        @pl.when((i >= 5) & (i < 5 + 2 * KEY_GROUPS) & (lax.rem(i, 2) == 1))
         def _():
             for g in range(key_group):
-                d = (i - 4) * key_group + g
+                d = (i - 5) // 2 * key_group + g
 
                 @pl.when(d > 0)
                 def _():
@@ -450,9 +488,9 @@
             own_part[piece] = sums[:piece_rows]
             pair_part[piece] = sums[piece_rows:]
 
-        @pl.when(jnp.logical_and(i >= 6, i < 6 + 2 * KEY_GROUPS))
-        def _():
-            block = i - 6
+        @pl.when(jnp.logical_and(i >= 7, i < 7 + 2 * KEY_GROUPS))
+        def _():
+            block = i - 7
 
             @pl.when(lax.rem(block, 2) == 0)
             def _():
@@ -483,11 +521,11 @@
                 def _():
                     leaving[m] = total
 
-                @pl.when(m >= pieces - 2)
-                def _():
-                    j = m - (pieces - 2)
-                    main_back[j] = total[:held_main].reshape(main_back.shape[1:])
-                    last_back[j] = total[held_main:]
+                for j in range(local_experts):
+
+                    @pl.when(m == pieces - 2 + j)
+                    def _(j=j):
+                        return_rows(j, total)
 
             @pl.when(m < pieces - 2)
             def _():
@@ -504,35 +542,12 @@
         return 0
 
     lax.fori_loop(0, pieces + 4, step, 0)
-    for copy in row_copies + head_copies:
-        copy.wait_send()
-
-    tiles = jnp.zeros((last_rows, LANES), F32)
-    for j in range(local_experts):
-        for c in range(column_tiles):
-            spot = place(last_rows, ep_count, j * column_tiles + c, local_experts * column_tiles)
-            tiles = tiles + matmul(spot, last_back[j, :, c * LANES : (c + 1) * LANES])
-    last_send[...] = tiles.astype(BF16).reshape(last_send.shape)
-    back_copies = exchange_copies(
-        "ep",
-        (lambda e: main_back.at[:, e], lambda e: last_send.at[e]),
-        (lambda e: main_recv.at[e], lambda e: last_recv.at[e]),
-        (main_back_sems.at[0], last_back_sems.at[0]),
-        (main_back_sems.at[1], last_back_sems.at[1]),
-    )
-    mixed_copies = exchange_copies(
-        "tp",
-        (lambda t: mixed_send.at[t],),
-        (lambda t: mixed_recv.at[t],),
-        (mixed_sems.at[0],),
-        (mixed_sems.at[1],),
-    )
-    for copy in back_copies + mixed_copies:
+    for copy in mixed_copies:
         copy.start()
     mixed_recv[tp_me] = mixed_send[tp_me]
-    last_recv[ep_me] = last_send[ep_me]
-    for j in range(local_experts):
-        main_recv[ep_me, j] = main_back[j, ep_me]
+    rows_recv[ep_me] = rows_back[ep_me]
+    for copy in row_copies[0] + row_copies[1] + head_copies:
+        copy.wait_send()
 
     def finish(i, _):
         @pl.when(i < pieces - 2)
@@ -569,13 +584,14 @@
         heads.append(jnp.where(lower, pltpu.roll(even, HEAD, 1), odd).astype(BF16))
     mix_out[...] = matmul(jnp.concatenate(heads, axis=1), w_out[...]).astype(BF16)
 
-    for copy in back_copies:
+    for copy in back_copies[0] + back_copies[1]:
         copy.wait()
-    results[:main_rows, :] = main_recv[...].reshape(main_rows, width)
-    tiles = last_recv[...].reshape(last_rows, LANES)
+    tiles = rows_recv[:, :, column_tiles].reshape(last_rows, LANES)
     for c in range(column_tiles):
+        columns = slice(c * LANES, (c + 1) * LANES)
+        results[:main_rows, columns] = rows_recv[:, :, c].reshape(main_rows, LANES)
         chosen = matmul(pick(experts, last_rows, c, column_tiles), tiles)
-        results[main_rows : main_rows + experts, c * LANES : (c + 1) * LANES] = chosen.astype(BF16)
+        results[main_rows : main_rows + experts, columns] = chosen.astype(BF16)
     combined = jnp.zeros((tokens, width), F32)
     for k, taker in enumerate(takers):
         row = jnp.broadcast_to(weights_ref[k : k + 1, :], (tokens, tokens))
@@ -594,9 +610,9 @@
     head = pltpu.VMEM((pieces, rows, LANES), BF16)
     query_tile = math.gcd(pieces * rows, 256)
     state = pltpu.VMEM((pieces * rows // query_tile, query_tile, LANES), F32)
-    by_device = pltpu.VMEM((ep_count, local_experts, capacity - 1, width), BF16)
-    by_expert = pltpu.VMEM((local_experts, ep_count, capacity - 1, width), BF16)
-    last = pltpu.VMEM((ep_count, local_experts * width // LANES, LANES), BF16)
+    column_tiles = width // LANES
+    assert column_tiles == capacity - 1
+    block = pltpu.VMEM((ep_count, local_experts, column_tiles + 1, capacity - 1, LANES), BF16)
     sums = pltpu.VMEM((pieces,) + piece, BF16)
     flights = pltpu.VMEM((pieces - 2,) + piece, BF16)
     result_rows = -(-local_experts * ep_count * capacity // LANES) * LANES
@@ -616,16 +632,15 @@
         scratch_shapes=[
             pltpu.VMEM(w.shape, BF16) for w in (w_query, w_key, w_value, w_out, w_gate, w_up, w_down)
         ]
-        + [head, head, by_device, by_expert, last, last]
+        + [head, head, block, block]
         + [pltpu.VMEM((pieces, 2) + piece, BF16), sums, sums, sums, flights, flights]
         + [pltpu.VMEM((2, ep_count, pieces, rows // 2, LANES), BF16), head, state, state, state]
-        + [head, head, by_expert, by_device]
-        + [pltpu.VMEM((local_experts, ep_count, width), BF16), last]
+        + [head, head, block, block]
         + [pltpu.VMEM((result_rows, width), BF16)]
-        + [DMA((7,)), DMA((2, pieces)), DMA((2, ep_count)), DMA((2, ep_count))]
+        + [DMA((7,)), DMA((2, pieces)), DMA((2, local_experts, ep_count))]
         + [DMA((2, pieces))] * 4
         + [DMA((2, ep_count))] * 2
-        + [DMA((2, pieces)), DMA((2, ep_count)), DMA((2, ep_count))],
+        + [DMA((2, pieces)), DMA((2, local_experts, ep_count))],
         name="layer",
         compiler_params=pltpu.CompilerParams(
             collective_id=0, has_side_effects=True, vmem_limit_bytes=62 * MIB

time: 139 us -> 128 us (0.921)
  Pallas kernels: 134 us -> 124 us
    pallas_call x1, Pallas kernels: 134 us -> 124 us  [layer(): pl.pallas_call(layer_body, out_shape=[jax.ShapeDtypeStruct((rows, w_out.s...]
where the time goes in v4:
time: 128 us
  Pallas kernels  124 us (97%)
  local copies, waits for them, and re-layouts  3.24 us (3%)
    pallas_call x1, Pallas kernels, layer(): pl.pallas_call(layer_body, out_shape=[jax.ShapeDtypeStruct((rows, w_out.s...  124 us
    unnamed x2, local copies, waits for them, and re-layouts  3.24 us

profile of v4, /device:TPU:1, one launch (start us, length us, event | category | flops | bytes accessed | tf_op | source)
XLA Modules:
  0.0 127.5 jit_solution(8922035803871710061)
XLA Ops:
  0.6 123.6 %layer.1 = (bf16[64,1024]{1,0:T(8,128)(2,1)}, bf16[128,1024]{1,0:T(8,128)(2,1)}) custom-call(bf16[64,1024]{1,0:T(8,128)(2,1)} %bitcast.8, f32[1,1024]{1,0:T(1,128)} %bitcast.10, bf16[1024,1024]{1,0:T(8,128)(2,1)} %query_hbm.1, bf16[1024,256]{1,0:T(8,128)(2,1)} %key_hbm.1, bf16[1024,256]{1,0:T(8,128)(2,1)} %value_hbm.1, f32[1,64]{1,0:T(1,128)} %bitcast.14, ...), custom_call_target="tpu_custom_call" | custom-call | tf_op jit(solution)/shard_map/layer/pallas_call | solution.py:619
  124.3 1.6 %copy.20 = bf16[64,1,1024]{2,0,1:T(8,128)(2,1)} copy(bf16[64,1,1024]{2,0,1:T(8,128)(2,1)} %bitcast.9) | data formatting | bytes 262144
  125.8 1.7 %copy.21 = bf16[128,1024]{1,0:T(8,128)(2,1)} copy(bf16[128,1024]{1,0:T(8,128)(2,1)} %get-tuple-element.9) | data formatting | bytes 524288

commit v5 on v4

--- a/solution.py
+++ b/solution.py
@@ -535,9 +535,14 @@
         def _():
             for tile in range(tiles_count):
                 mixed = row_acc[tile] / jnp.sum(row_sum[tile], axis=1, keepdims=True)
-                mixed_send[tile * tile_groups : (tile + 1) * tile_groups] = mixed.astype(
-                    BF16
-                ).reshape(tile_groups, rows, LANES)
+                mixed = mixed.reshape(tile_groups, rows, LANES)
+                first = mixed[:, :half].reshape(tile_groups * half, LANES)
+                second = mixed[:, half:].reshape(tile_groups * half, LANES)
+                upper = iota(first.shape, 1) >= HEAD
+                mixed = jnp.where(upper, second, pltpu.roll(first, HEAD, 1)).astype(BF16)
+                mixed_send[tile * tile_groups : (tile + 1) * tile_groups] = mixed.reshape(
+                    tile_groups, half, LANES
+                )
 
         return 0
 
@@ -581,7 +586,9 @@
     heads = []
     for t in range(tp_count // 2):
         even, odd = mixed_recv[2 * t].astype(F32), mixed_recv[2 * t + 1].astype(F32)
-        heads.append(jnp.where(lower, pltpu.roll(even, HEAD, 1), odd).astype(BF16))
+        first = jnp.where(lower_half, even, pltpu.roll(odd, HEAD, 1))
+        second = jnp.where(lower_half, pltpu.roll(even, HEAD, 1), odd)
+        heads.append(jnp.concatenate([first, second], axis=0).astype(BF16))
     mix_out[...] = matmul(jnp.concatenate(heads, axis=1), w_out[...]).astype(BF16)
 
     for copy in back_copies[0] + back_copies[1]:
@@ -608,6 +615,7 @@
     local_experts = w_gate.shape[0]
     piece = (ep_count * capacity, width)
     head = pltpu.VMEM((pieces, rows, LANES), BF16)
+    packed = pltpu.VMEM((pieces, rows // 2, LANES), BF16)
     query_tile = math.gcd(pieces * rows, 256)
     state = pltpu.VMEM((pieces * rows // query_tile, query_tile, LANES), F32)
     column_tiles = width // LANES
@@ -635,7 +643,7 @@
         + [head, head, block, block]
         + [pltpu.VMEM((pieces, 2) + piece, BF16), sums, sums, sums, flights, flights]
         + [pltpu.VMEM((2, ep_count, pieces, rows // 2, LANES), BF16), head, state, state, state]
-        + [head, head, block, block]
+        + [packed, packed, block, block]
         + [pltpu.VMEM((result_rows, width), BF16)]
         + [DMA((7,)), DMA((2, pieces)), DMA((2, local_experts, ep_count))]
         + [DMA((2, pieces))] * 4

time: 128 us -> 126 us (0.984)
  Pallas kernels: 124 us -> 122 us
    pallas_call x1, Pallas kernels: 124 us -> 122 us  [layer(): pl.pallas_call(layer_body, out_shape=[jax.ShapeDtypeStruct((rows, w_out.s...]
where the time goes in v5:
time: 126 us
  Pallas kernels  122 us (97%)
  local copies, waits for them, and re-layouts  3.24 us (3%)
    pallas_call x1, Pallas kernels, layer(): pl.pallas_call(layer_body, out_shape=[jax.ShapeDtypeStruct((rows, w_out.s...  122 us
    unnamed x2, local copies, waits for them, and re-layouts  3.24 us

profile of v5, /device:TPU:1, one launch (start us, length us, event | category | flops | bytes accessed | tf_op | source)
XLA Modules:
  0.0 125.9 jit_solution(2274909724947783922)
XLA Ops:
  0.6 122.0 %layer.1 = (bf16[64,1024]{1,0:T(8,128)(2,1)}, bf16[128,1024]{1,0:T(8,128)(2,1)}) custom-call(bf16[64,1024]{1,0:T(8,128)(2,1)} %bitcast.8, f32[1,1024]{1,0:T(1,128)} %bitcast.10, bf16[1024,1024]{1,0:T(8,128)(2,1)} %query_hbm.1, bf16[1024,256]{1,0:T(8,128)(2,1)} %key_hbm.1, bf16[1024,256]{1,0:T(8,128)(2,1)} %value_hbm.1, f32[1,64]{1,0:T(1,128)} %bitcast.14, ...), custom_call_target="tpu_custom_call" | custom-call | tf_op jit(solution)/shard_map/layer/pallas_call | solution.py:627
  122.7 1.6 %copy.20 = bf16[64,1,1024]{2,0,1:T(8,128)(2,1)} copy(bf16[64,1,1024]{2,0,1:T(8,128)(2,1)} %bitcast.9) | data formatting | bytes 262144
  124.2 1.7 %copy.21 = bf16[128,1024]{1,0:T(8,128)(2,1)} copy(bf16[128,1024]{1,0:T(8,128)(2,1)} %get-tuple-element.9) | data formatting | bytes 524288
